TPU v7x, 32 devices: a whole 2x2x4 slice. The times are simulated.
32 devices in a mesh: sp: 8 (over z, x), tp: 4 (over y, core).
Axes of the slice: x: 2, y: 2, z: 4, core: 2. Of those that a mesh axis runs over, the one named last changes fastest.
Arguments:
- residual: bfloat16 [3072, 2048], P('sp', 'tp'), may hold values from -6 to 6
- query_nope: bfloat16 [3072, 4096], P('sp', 'tp'), may hold values from -9 to 9
- query_rope: bfloat16 [3072, 2048], P('sp', 'tp'), may hold values from -600 to 600
- latent: bfloat16 [3072, 512], P('sp'), may hold values from -6 to 6
- rope_key: bfloat16 [3072, 64], P('sp'), may hold values from -6 to 6
- doc_ids: int32 [3072], P('sp'), may hold values from 0 to 3, never falling along the last dimension, each value on 1 to 1152 neighbouring positions
- key_up: bfloat16 [512, 4096], P(None, 'tp'), may hold values from -0.25 to 0.25
- value_up: bfloat16 [512, 4096], P(None, 'tp'), may hold values from -0.25 to 0.25
- out_proj: bfloat16 [4096, 2048], P('tp'), may hold values from -0.375 to 0.375
- norm1_gain: bfloat16 [2048], P('tp'), may hold values from 0.099609375 to 1.8984375
- norm1_bias: bfloat16 [2048], P('tp'), may hold values from -3 to 3
- ffn_gate: bfloat16 [2048, 5632], P('sp', 'tp'), may hold values from -0.125 to 0.125
- ffn_value: bfloat16 [2048, 5632], P('sp', 'tp'), may hold values from -0.125 to 0.125
- conv_gate: bfloat16 [3, 5632], P(None, 'tp'), may hold values from -3.5 to 3.5
- conv_value: bfloat16 [3, 5632], P(None, 'tp'), may hold values from -3.5 to 3.5
- ffn_down: bfloat16 [5632, 2048], P('tp', 'sp'), may hold values from -0.15625 to 0.15625
- norm2_gain: bfloat16 [2048], P('tp'), may hold values from 0.099609375 to 1.8984375
- norm2_bias: bfloat16 [2048], P('tp'), may hold values from -3 to 3
Outputs:
- layer_out: bfloat16 [3072, 2048], P('sp', 'tp')
Inputs may be any that keep to these rules, and one draw needn't show every extreme that they name: `doc_ids`: document numbers never fall along the positions; each document holds 1 to 1152 positions, and one holds exactly 1152.
All inputs are finite; a program needn't handle non-finite values.
Results may differ from a plain program's by a relative error of at most 0.014.
Values may be sent and summed in bfloat16 or wider, within the bound.
A program may use at most 128 MiB of HBM per device.

v0:
```python
import functools

import jax
import jax.numpy as jnp
from jax import lax
from jax.experimental import pallas as pl
from jax.experimental.pallas import tpu as pltpu
from jax.sharding import PartitionSpec as P

D = 2048
NOPE = 128
ROPE = 64
VDIM = 128
CONV = 3
REACH = 3


norm_eps = 1e-05
residual_scale = 8.0**0.25
rope_base_freq = 10000.0
masked_score = -1e30


def passed_along(value, axis, by):
    count = lax.axis_size(axis)
    pairs = [(i, i + by) for i in range(count) if 0 <= i + by < count]
    return lax.ppermute(value, axis, pairs)


def tables(positions):
    frequencies = 1.0 / rope_base_freq ** (jnp.arange(0, ROPE, 2, dtype=jnp.float32) / ROPE)
    angles = positions.astype(jnp.float32)[:, None] * frequencies[None, :]
    return (jnp.cos(angles), jnp.sin(angles))


def rotate(vectors, cosine, sine_table):
    half_width = vectors.shape[-1] // 2
    front_half = vectors[..., :half_width]
    back_half = vectors[..., half_width:]
    return jnp.concatenate(
        [
            front_half * cosine - back_half * sine_table,
            front_half * sine_table + back_half * cosine,
        ],
        axis=-1,
    )


def ring_blocks(block, axis):
    count = lax.axis_size(axis)
    order = list(range(0, count, 2)) + list(range(1, count, 2))[::-1]
    place = [order.index(i) for i in range(count)]
    me = lax.axis_index(axis)
    found = [(me, block)]
    ahead = count // 2
    for turn, steps in ((1, ahead), (-1, count - 1 - ahead)):
        pairs = [(order[p], order[(p + turn) % count]) for p in range(count)]
        moving = block
        for step in range(1, steps + 1):
            moving = lax.ppermute(moving, axis, pairs)
            owners = [order[(place[i] - turn * step) % count] for i in range(count)]
            found.append((jnp.asarray(owners, jnp.int32)[me], moving))
    return found


def attend_kernel(chunk, reach_rows, scale, q_ref, turned_ref, k_ref, rope_ref, v_ref, bias_ref, out_ref):
    rows = q_ref.shape[0]
    span = chunk + reach_rows
    rope_rows = rope_ref[...]
    for head in range(q_ref.shape[1] // NOPE):
        nope = slice(head * NOPE, (head + 1) * NOPE)
        rope = slice(head * ROPE, (head + 1) * ROPE)
        queries = jnp.concatenate([q_ref[:, nope], turned_ref[:, rope]], 1)
        keys = jnp.concatenate([k_ref[:, nope], rope_rows], 1)
        for start in range(0, rows, chunk):
            cut = slice(start, start + chunk)
            seen = slice(start, start + span)
            scores = lax.dot_general(
                queries[cut], keys[seen], (((1,), (1,)), ((), ())), preferred_element_type=jnp.float32
            )
            scores = scores * scale + bias_ref[cut, seen]
            weights = jnp.exp(scores - jnp.max(scores, -1, keepdims=True))
            weights = weights * (1.0 / jnp.sum(weights, -1, keepdims=True))
            out_ref[cut, nope] = jnp.dot(
                weights.astype(jnp.bfloat16), v_ref[seen, nope], preferred_element_type=jnp.float32
            ).astype(jnp.bfloat16)


def attend(queries, turned, keys, rope_rows, values, bias, scale):
    rows, width = queries.shape
    window = keys.shape[0]
    chunk = 128 if rows % 128 == 0 else rows
    pair = 2
    wide = pair * NOPE
    heads = width // NOPE
    return pl.pallas_call(
        functools.partial(attend_kernel, chunk, window - rows, scale),
        grid=(heads // pair,),
        in_specs=[
            pl.BlockSpec((rows, wide), lambda i: (0, i)),
            pl.BlockSpec((rows, pair * ROPE), lambda i: (0, i)),
            pl.BlockSpec((window, wide), lambda i: (0, i)),
            pl.BlockSpec((window, ROPE), lambda i: (0, 0)),
            pl.BlockSpec((window, pair * VDIM), lambda i: (0, i)),
            pl.BlockSpec((rows, window), lambda i: (0, 0)),
        ],
        out_specs=pl.BlockSpec((rows, pair * VDIM), lambda i: (0, i)),
        out_shape=jax.ShapeDtypeStruct((rows, heads * VDIM), jnp.bfloat16),
        compiler_params=pltpu.CompilerParams(vmem_limit_bytes=40 * 1024 * 1024),
        cost_estimate=pl.CostEstimate(
            flops=16 * rows * window * heads * (NOPE + ROPE + VDIM),
            bytes_accessed=2 * (4 * rows * width + 2 * window * width),
            transcendentals=rows * window * heads,
        ),
    )(queries, turned, keys, rope_rows, values, bias)


def scatter_sum(terms, axis):
    count = lax.axis_size(axis)
    width = terms.shape[1] // count
    parts = jnp.stack([terms[:, i * width : (i + 1) * width] for i in range(count)])
    got = lax.all_to_all(parts.astype(jnp.bfloat16), axis, 0, 0)
    return jnp.sum(got.astype(jnp.float32), 0)


def finish(mixed, totals, gain_row, bias_row):
    row_mean = totals[0][:, None] / D
    row_power = totals[1][:, None] / D
    return (mixed - row_mean) * lax.rsqrt(
        row_power - row_mean * row_mean + norm_eps
    ) * gain_row.astype(jnp.float32) + bias_row.astype(jnp.float32)


def local(
    residual,
    query_nope,
    query_rope,
    latent,
    rope_key,
    doc_ids,
    key_up,
    value_up,
    out_proj,
    norm1_gain,
    norm1_bias,
    ffn_gate,
    ffn_value,
    conv_gate,
    conv_value,
    ffn_down,
    norm2_gain,
    norm2_bias,
):
    row_count = latent.shape[0]
    head_count = query_nope.shape[1] // NOPE
    local_units = ffn_gate.shape[1]
    rim_rows = CONV - 1
    whole_gate = lax.all_gather(ffn_gate, "sp", axis=0, tiled=True)
    whole_value = lax.all_gather(ffn_value, "sp", axis=0, tiled=True)
    offset = lax.axis_index("sp") * row_count
    positions = offset + jnp.arange(row_count, dtype=jnp.int32)
    cosine, sine_table = tables(positions)
    turned_key = rotate(rope_key.astype(jnp.float32), cosine, sine_table).astype(jnp.bfloat16)
    turned_query = rotate(
        query_rope.astype(jnp.float32).reshape(row_count, head_count, ROPE),
        cosine[:, None],
        sine_table[:, None],
    ).astype(jnp.bfloat16)
    latent_width = latent.shape[1]
    packed = jnp.concatenate(
        [
            latent,
            turned_key,
            jnp.broadcast_to(doc_ids.astype(jnp.bfloat16)[:, None], (row_count, ROPE)),
        ],
        1,
    )
    parts = [passed_along(packed, "sp", shift_step) for shift_step in range(REACH, 0, -1)]
    pieces = jnp.concatenate(parts + [packed], 0)
    win_latent = pieces[:, :latent_width]
    win_key = pieces[:, latent_width : latent_width + ROPE]
    win_doc = pieces[:, latent_width + ROPE].astype(jnp.int32)
    down_blocks = ring_blocks(ffn_down, "sp")
    key_rows = jnp.dot(win_latent, key_up, preferred_element_type=jnp.float32).astype(jnp.bfloat16)
    values = jnp.dot(win_latent, value_up, preferred_element_type=jnp.float32).astype(jnp.bfloat16)
    window = key_rows.shape[0]
    key_pos = offset - REACH * row_count + jnp.arange(window, dtype=jnp.int32)
    allowed = (
        (key_pos[None, :] <= positions[:, None])
        & (key_pos[None, :] >= 0)
        & (win_doc[None, :] == doc_ids[:, None])
    )
    scale = (NOPE + ROPE) ** (-0.5)
    bias = jnp.where(allowed, 0.0, masked_score).astype(jnp.float32)
    attended = attend(
        query_nope,
        turned_query.reshape(row_count, head_count * ROPE),
        key_rows,
        win_key,
        values,
        bias,
        scale,
    )
    head_terms = jnp.dot(attended, out_proj, preferred_element_type=jnp.float32)
    projected = scatter_sum(head_terms, "tp")
    mixed_one = residual_scale * residual.astype(jnp.float32) + projected
    totals_one = lax.psum((jnp.sum(mixed_one, 1), jnp.sum(mixed_one * mixed_one, 1)), "tp")
    normed = finish(mixed_one, totals_one, norm1_gain, norm1_bias).astype(jnp.bfloat16)
    half = row_count // 2
    full_rows = jnp.concatenate(
        [
            lax.all_gather(normed[:half], "tp", axis=1, tiled=True),
            lax.all_gather(normed[half:], "tp", axis=1, tiled=True),
        ],
        0,
    )
    gate_sum = jnp.dot(full_rows, whole_gate, preferred_element_type=jnp.float32)
    value_sum = jnp.dot(full_rows, whole_value, preferred_element_type=jnp.float32)
    gate_pre = gate_sum.astype(jnp.bfloat16)
    value_pre = value_sum.astype(jnp.bfloat16)
    tail_gate, tail_value, tail_doc = passed_along(
        (
            gate_pre[row_count - rim_rows :],
            value_pre[row_count - rim_rows :],
            doc_ids[row_count - rim_rows :],
        ),
        "sp",
        1,
    )
    ext_gate = jnp.concatenate([tail_gate, gate_pre], 0)
    ext_value = jnp.concatenate([tail_value, value_pre], 0)
    ext_doc = jnp.concatenate([tail_doc, doc_ids], 0)
    gate_mix = jnp.zeros((row_count, local_units), jnp.float32)
    value_mix = jnp.zeros((row_count, local_units), jnp.float32)
    for tap_index in range(CONV):
        valid_tap = (
            (ext_doc[tap_index : tap_index + row_count] == doc_ids)
            & (positions - rim_rows + tap_index >= 0)
        ).astype(jnp.float32)[:, None]
        gate_mix = (
            gate_mix
            + conv_gate[tap_index].astype(jnp.float32)
            * ext_gate[tap_index : tap_index + row_count].astype(jnp.float32)
            * valid_tap
        )
        value_mix = (
            value_mix
            + conv_value[tap_index].astype(jnp.float32)
            * ext_value[tap_index : tap_index + row_count].astype(jnp.float32)
            * valid_tap
        )
    hidden = (value_mix * jax.nn.gelu(gate_mix)).astype(jnp.bfloat16)
    sp_count = lax.axis_size("sp")
    tp_count = lax.axis_size("tp")
    block_width = ffn_down.shape[1]
    unit_terms = jnp.zeros((sp_count, row_count, block_width), jnp.bfloat16)
    for owner, block in down_blocks:
        term = jnp.dot(hidden, block, preferred_element_type=jnp.float32).astype(jnp.bfloat16)
        unit_terms = lax.dynamic_update_slice(unit_terms, term[None], (owner, 0, 0))
    share = sp_count // tp_count
    got = lax.all_to_all(
        unit_terms.reshape(tp_count, share, row_count, block_width), "tp", 0, 0
    )
    ffn_blocks = jnp.sum(got.astype(jnp.float32), 0)
    ffn_out = jnp.concatenate([ffn_blocks[i] for i in range(share)], 1)
    mixed_two = residual_scale * normed.astype(jnp.float32) + ffn_out
    totals_two = lax.psum((jnp.sum(mixed_two, 1), jnp.sum(mixed_two * mixed_two, 1)), "tp")
    return finish(mixed_two, totals_two, norm2_gain, norm2_bias).astype(jnp.bfloat16)


def solution(mesh):
    placed = (
        P("sp", "tp"),
        P("sp", "tp"),
        P("sp", "tp"),
        P("sp", None),
        P("sp", None),
        P("sp"),
        P(None, "tp"),
        P(None, "tp"),
        P("tp", None),
        P("tp"),
        P("tp"),
        P("sp", "tp"),
        P("sp", "tp"),
        P(None, "tp"),
        P(None, "tp"),
        P("tp", "sp"),
        P("tp"),
        P("tp"),
    )
    return jax.shard_map(
        local, mesh=mesh, in_specs=placed, out_specs=P("sp", "tp"), check_vma=False
    )
```

profile of v0, /device:TPU:21, one launch (start us, length us, event | category | flops | bytes accessed | tf_op | source)
XLA Modules:
  0.0 325.6 jit_solution(16483978702596401627)
XLA Ops:
  6.5 0.7 all-gather.5.cloned.1.call-update
  7.3 0.7 all-gather.3.cloned.1.call-update
  8.0 0.9 copy.36
  9.0 0.7 convert_element_type.147
  9.7 1.6 subtract_convert_fusion.1
  11.4 0.9 pad_maximum_fusion.3
  12.3 3.1 collective-permute-start.2
  15.5 3.2 collective-permute-start.1
  18.7 1.9 collective-permute-start
  20.7 1.2 copy.32
  21.9 1.0 convert.39
  22.8 1.0 copy.35
  23.9 1.0 copy.34
  24.9 1.2 subtract_convert_fusion
  26.1 0.8 pad_maximum_fusion.4
  26.9 1.2 copy.37.turned_ref
  28.1 8.4 %collective-permute-done.2 = bf16[384,640]{1,0:T(8,128)(2,1)S(1)} collective-permute-done((bf16[384,640]{1,0:T(8,128)(2,1)}, bf16[384,640]{1,0:T(8,128)(2,1)S(1)}, u32[]{:S(2)}, u32[]{:S(2)}) %collective-permute-start.2) | collective-permute-done | bytes 491552 | tf_op jit(solution)/shard_map/ppermute | solution.py:27
  36.6 10.3 %collective-permute-done.1 = bf16[384,640]{1,0:T(8,128)(2,1)S(1)} collective-permute-done((bf16[384,640]{1,0:T(8,128)(2,1)}, bf16[384,640]{1,0:T(8,128)(2,1)S(1)}, u32[]{:S(2)}, u32[]{:S(2)}) %collective-permute-start.1) | collective-permute-done | bytes 491552 | tf_op jit(solution)/shard_map/ppermute | solution.py:27
  46.9 24.7 %collective-permute-done = bf16[384,640]{1,0:T(8,128)(2,1)S(1)} collective-permute-done((bf16[384,640]{1,0:T(8,128)(2,1)}, bf16[384,640]{1,0:T(8,128)(2,1)S(1)}, u32[]{:S(2)}, u32[]{:S(2)}) %collective-permute-start) | collective-permute-done | bytes 491552 | tf_op jit(solution)/shard_map/ppermute | solution.py:27
  71.6 1.3 convert_reduce_fusion.2
  73.0 7.1 %maximum_maximum_fusion = bf16[1536,640]{1,0:T(8,128)(2,1)S(1)} fusion(bf16[384,64]{1,0:T(8,128)(2,1)S(1)} %copy-done.7, bf16[384,32]{1,0:T(8,128)(2,1)S(1)} %get-tuple-element.30, bf16[384,32]{1,0:T(8,128)(2,1)S(1)} %get-tuple-element.29, bf16[384,512]{1,0:T(8,128)(2,1)S(1)} %copy-done.5, bf16[384,640]{1,0:T(8,128)(2,1)S(1)} %collective-permute-done.2, ...), kind=kLoop, calls=%fused_computation.18 | loop fusion | flops 13762560 | bytes 3932160 | tf_op jit(solution)/shard_map/concatenate | solution.py:179
  80.2 1.8 convolution_convert_fusion.1.k_ref
  82.0 1.8 convolution_convert_fusion.v_ref
  83.8 0.7 and_select_fusion.bias_ref
  85.0 17.2 %shard_map.235 = bf16[384,1024]{1,0:T(8,128)(2,1)S(1)} custom-call(bf16[384,1024]{1,0:T(8,128)(2,1)S(1)} %copy-done.1, bf16[384,512]{1,0:T(8,128)(2,1)S(1)} %copy.37.turned_ref, bf16[1536,1024]{1,0:T(8,128)(2,1)S(1)} %convolution_convert_fusion.1.k_ref, bf16[1536,64]{1,0:T(8,128)(2,1)S(1)} %maximum_maximum_fusion.1.rope_ref, ...), custom_call_target="tpu_custom_call" | custom-call | flops 24159191040 | bytes 9437184 | tf_op jit(solution)/shard_map/pallas_call | solution.py:96
  102.2 1.8 convolution_convert_fusion.4
  104.1 1.4 pad_maximum_fusion
  105.6 5.4 %all-to-all-start = ((bf16[4,384,512]{2,1,0:T(8,128)(2,1)}), bf16[4,384,512]{2,1,0:T(8,128)(2,1)S(1)}, u32[]{:S(2)}, u32[]{:S(2)}) async-start(bf16[4,384,512]{2,1,0:T(8,128)(2,1)} %pad_maximum_fusion), calls=%async_computation | async-start | bytes 3145728 | tf_op jit(solution)/shard_map/all_to_all | solution.py:122
  111.0 41.3 %collective-permute-start.7 = (bf16[1408,256]{1,0:T(8,128)(2,1)}, bf16[1408,256]{1,0:T(8,128)(2,1)}, u32[]{:S(2)}, u32[]{:S(2)}) collective-permute-start(bf16[1408,256]{1,0:T(8,128)(2,1)} %collective-permute-done.6), channel_id=1, source_target_pairs={{0,8},{8,16},{16,24},{24,28},{28,20},{20,12},{12,4},{4,0},{1,9},{9... | collective-permute-start | bytes 2162696 | tf_op jit(solution)/shard_map/ppermute | solution.py:60
  152.3 1.9 collective-permute-start.4
  156.2 0.6 dynamic_slice.22
  158.1 0.6 dynamic_slice.23
  161.6 0.6 dynamic_slice.25
  163.4 0.6 dynamic_slice.26
  165.3 0.6 dynamic_slice.27
  171.5 13.9 %collective-permute-done.4 = s32[2]{0:T(128)S(1)} collective-permute-done((s32[2]{0:T(128)S(1)}, s32[2]{0:T(128)S(1)}, u32[]{:S(2)}, u32[]{:S(2)}) %collective-permute-start.4) | collective-permute-done | bytes 40 | tf_op jit(solution)/shard_map/ppermute | solution.py:27
  185.5 3.9 %collective-permute-done.7 = bf16[1408,256]{1,0:T(8,128)(2,1)} collective-permute-done((bf16[1408,256]{1,0:T(8,128)(2,1)}, bf16[1408,256]{1,0:T(8,128)(2,1)}, u32[]{:S(2)}, u32[]{:S(2)}) %collective-permute-start.7) | collective-permute-done | bytes 720928 | tf_op jit(solution)/shard_map/ppermute | solution.py:60
  189.4 2.2 collective-permute-start.8
  191.8 1.2 fusion.29
  193.0 5.8 %all-reduce.1 = (f32[384]{0:T(512)S(1)}, f32[384]{0:T(512)S(1)}) all-reduce(f32[384]{0:T(512)S(1)} %get-tuple-element.8, f32[384]{0:T(512)S(1)} %get-tuple-element.7), channel_id=1, replica_groups=mesh['sp'=8,'tp'=4] {'tp'}, use_global_device_ids=true, to_apply=%region_4.5 | all-reduce | flops 768 | bytes 6144 | tf_op jit(solution)/shard_map/psum | solution.py:207
  198.9 1.2 add_convert_fusion.1
  200.2 9.3 %all_gather.12 = bf16[192,2048]{1,0:T(8,128)(2,1)S(1)} all-gather(bf16[192,512]{1,0:T(8,128)(2,1)S(1)} %get-tuple-element.28), channel_id=1, replica_groups=mesh['sp'=8,'tp'=4] {'tp'}, dimensions={1}, use_global_device_ids=true | all-gather | bytes 983040 | tf_op jit(solution)/shard_map/all_gather | solution.py:212
  209.5 1.0 constant_dynamic-update-slice_fusion.1
  210.5 8.7 %all_gather.13 = bf16[192,2048]{1,0:T(8,128)(2,1)S(1)} all-gather(bf16[192,512]{1,0:T(8,128)(2,1)S(1)} %get-tuple-element.27), channel_id=1, replica_groups=mesh['sp'=8,'tp'=4] {'tp'}, dimensions={1}, use_global_device_ids=true | all-gather | bytes 983040 | tf_op jit(solution)/shard_map/all_gather | solution.py:213
  219.2 1.0 constant_dynamic-update-slice_fusion
  220.2 5.7 %convolution_convert_fusion.2 = bf16[384,1408]{1,0:T(8,128)(2,1)S(1)} fusion(bf16[384,2048]{1,0:T(8,128)(2,1)} %constant_dynamic-update-slice_fusion, bf16[2048,1408]{1,0:T(8,128)(2,1)} %all-gather.5.cloned.1.call-done), kind=kOutput, calls=%fused_computation.5 | convolution fusion | flops 2215133184 | bytes 8421376 | tf_op jit(solution)/shard_map/dot_general | solution.py:217
  225.9 1.9 collective-permute-start.5
  227.8 26.3 %all-gather.3.cloned.1.call-done = bf16[2048,1408]{1,0:T(8,128)(2,1)} async-done(((bf16[256,1408]{1,0:T(8,128)(2,1)}), bf16[2048,1408]{1,0:T(8,128)(2,1)}) %all-gather.3.cloned.1.call-update) | async-done | bytes 5767184 | tf_op jit(solution)/shard_map/all_gather | solution.py:159
  254.1 5.7 %convolution_convert_fusion.3 = bf16[384,1408]{1,0:T(8,128)(2,1)S(1)} fusion(bf16[384,2048]{1,0:T(8,128)(2,1)} %constant_dynamic-update-slice_fusion, bf16[2048,1408]{1,0:T(8,128)(2,1)} %all-gather.3.cloned.1.call-done), kind=kOutput, calls=%fused_computation.6 | convolution fusion | flops 2215133184 | bytes 8421376 | tf_op jit(solution)/shard_map/dot_general | solution.py:218
  259.9 5.5 %collective-permute-start.3 = (bf16[2,1408]{1,0:T(2,128)(2,1)S(1)}, bf16[2,1408]{1,0:T(2,128)(2,1)S(1)}, u32[]{:S(2)}, u32[]{:S(2)}) collective-permute-start(bf16[2,1408]{1,0:T(2,128)(2,1)S(1)} %slice.135), channel_id=1, source_target_pairs={{0,4},{4,8},{8,12},{12,16},{16,20},{20,24},{24,28},{1,5},{5,9},{9,... | collective-permute-start | bytes 16904 | tf_op jit(solution)/shard_map/ppermute | solution.py:27
  265.5 1.4 collective-permute-start.9
  266.9 3.2 fusion.8
  270.2 1.6 fusion.12
  271.8 1.6 fusion.14
  273.4 1.6 fusion.16
  275.0 1.6 fusion.18
  276.6 5.4 %collective-permute-done.9 = bf16[1408,256]{1,0:T(8,128)(2,1)S(1)} collective-permute-done((bf16[1408,256]{1,0:T(8,128)(2,1)}, bf16[1408,256]{1,0:T(8,128)(2,1)S(1)}, u32[]{:S(2)}, u32[]{:S(2)}) %collective-permute-start.9) | collective-permute-done | bytes 720928 | tf_op jit(solution)/shard_map/ppermute | solution.py:60
  282.5 1.6 fusion.22
  284.1 1.6 fusion.24
  286.2 1.2 copy-done.2
  287.4 6.1 %all-to-all-start.1 = ((bf16[4,2,384,256]{3,2,1,0:T(8,128)(2,1)}), bf16[4,2,384,256]{3,2,1,0:T(8,128)(2,1)S(1)}, u32[]{:S(2)}, u32[]{:S(2)}) async-start(bf16[4,2,384,256]{3,2,1,0:T(8,128)(2,1)} %bitcast.79), calls=%async_computation.1 | async-start | bytes 3145728 | tf_op jit(solution)/shard_map/all_to_all | solution.py:261
  293.5 18.2 %all-to-all-done.1 = bf16[4,2,384,256]{3,2,1,0:T(8,128)(2,1)S(1)} async-done(((bf16[4,2,384,256]{3,2,1,0:T(8,128)(2,1)}), bf16[4,2,384,256]{3,2,1,0:T(8,128)(2,1)S(1)}, u32[]{:S(2)}, u32[]{:S(2)}) %all-to-all-start.1) | async-done | bytes 1572896 | tf_op jit(solution)/shard_map/all_to_all | solution.py:261
  312.2 5.6 %all-reduce = (f32[384]{0:T(512)S(1)}, f32[384]{0:T(512)S(1)}) all-reduce(f32[384]{0:T(512)S(1)} %get-tuple-element.6, f32[384]{0:T(512)S(1)} %get-tuple-element.5), channel_id=1, replica_groups=mesh['sp'=8,'tp'=4] {'tp'}, use_global_device_ids=true, to_apply=%region_9.10 | all-reduce | flops 768 | bytes 6144 | tf_op jit(solution)/shard_map/psum | solution.py:267
  317.8 1.0 add_convert_fusion
  (94 shorter events, 4.4 us)
Async XLA Ops:
  6.5 73.6 %copy-start = (bf16[512,1024]{1,0:T(8,128)(2,1)S(1)}, bf16[512,1024]{1,0:T(8,128)(2,1)}, u32[]{:S(2)}) copy-start(bf16[512,1024]{1,0:T(8,128)(2,1)} %param.31) | copy-start | bytes 3145732
  6.5 4.8 %copy-start.5 = (bf16[384,512]{1,0:T(8,128)(2,1)S(1)}, bf16[384,512]{1,0:T(8,128)(2,1)}, u32[]{:S(2)}) copy-start(bf16[384,512]{1,0:T(8,128)(2,1)} %param.28) | copy-start | bytes 1179652
  6.5 213.6 %all-gather.5.cloned.1.call-start = ((), (), s32[]{:S(2)}) async-start(), calls=%async_computation.3 | async-start | bytes 6488064 | tf_op jit(solution)/shard_map/all_gather | solution.py:158
  7.3 246.9 %all-gather.3.cloned.1.call-start = ((), (), s32[]{:S(2)}) async-start(), calls=%async_computation.2 | async-start | bytes 6488064 | tf_op jit(solution)/shard_map/all_gather | solution.py:159
  11.4 4.1 %copy-start.6 = (bf16[384,64]{1,0:T(8,128)(2,1)}, bf16[384,64]{1,0:T(8,128)(2,1)S(1)}, u32[]{:S(2)}) copy-start(bf16[384,64]{1,0:T(8,128)(2,1)S(1)} %broadcast_in_dim.28) | copy-start | bytes 147460
  12.3 24.2 %collective-permute-start.2 = (bf16[384,640]{1,0:T(8,128)(2,1)}, bf16[384,640]{1,0:T(8,128)(2,1)S(1)}, u32[]{:S(2)}, u32[]{:S(2)}) collective-permute-start(bf16[384,640]{1,0:T(8,128)(2,1)} %pad_maximum_fusion.3), channel_id=1, source_target_pairs={{0,4},{4,8},{8,12},{12,16},{16,20},{20,24},{24,28},{1,5},{5,9},{9,... | collective-permute-start | bytes 1474568 | tf_op jit(solution)/shard_map/ppermute | solution.py:27
  15.5 31.4 %collective-permute-start.1 = (bf16[384,640]{1,0:T(8,128)(2,1)}, bf16[384,640]{1,0:T(8,128)(2,1)S(1)}, u32[]{:S(2)}, u32[]{:S(2)}) collective-permute-start(bf16[384,640]{1,0:T(8,128)(2,1)} %pad_maximum_fusion.3), channel_id=1, source_target_pairs={{0,8},{4,12},{8,16},{12,20},{16,24},{20,28},{1,9},{5,13},{9,17},{1... | collective-permute-start | bytes 1474568 | tf_op jit(solution)/shard_map/ppermute | solution.py:27
  18.7 52.9 %collective-permute-start = (bf16[384,640]{1,0:T(8,128)(2,1)}, bf16[384,640]{1,0:T(8,128)(2,1)S(1)}, u32[]{:S(2)}, u32[]{:S(2)}) collective-permute-start(bf16[384,640]{1,0:T(8,128)(2,1)} %pad_maximum_fusion.3), channel_id=1, source_target_pairs={{0,12},{4,16},{8,20},{12,24},{16,28},{1,13},{5,17},{9,21},{13,25},... | collective-permute-start | bytes 1474568 | tf_op jit(solution)/shard_map/ppermute | solution.py:27
  20.6 90.4 %collective-permute-start.6 = (bf16[1408,256]{1,0:T(8,128)(2,1)}, bf16[1408,256]{1,0:T(8,128)(2,1)}, u32[]{:S(2)}, u32[]{:S(2)}) collective-permute-start(bf16[1408,256]{1,0:T(8,128)(2,1)} %param.40), channel_id=1, source_target_pairs={{0,8},{8,16},{16,24},{24,28},{28,20},{20,12},{12,4},{4,0},{1,9},{9... | collective-permute-start | bytes 2162696 | tf_op jit(solution)/shard_map/ppermute | solution.py:60
  28.1 44.8 %copy-start.7 = (bf16[384,64]{1,0:T(8,128)(2,1)S(1)}, bf16[384,64]{1,0:T(8,128)(2,1)}, u32[]{:S(2)}) copy-start(bf16[384,64]{1,0:T(8,128)(2,1)} %copy-done.6) | copy-start | bytes 147460
  80.2 1.8 copy-start.16
  82.0 1.8 copy-start.8
  83.8 1.1 copy-start.1
  85.0 17.2 %copy-start.15 = (bf16[1024,2048]{1,0:T(8,128)(2,1)S(1)}, bf16[1024,2048]{1,0:T(8,128)(2,1)}, u32[]{:S(2)}) copy-start(bf16[1024,2048]{1,0:T(8,128)(2,1)} %param.33) | copy-start | bytes 12582916
  105.5 48.7 %copy-start.23 = (s32[8]{0:T(128)S(1)}, s32[8]{0:T(128)}, u32[]{:S(2)}) copy-start(s32[8]{0:T(128)} %constant.70.clone) | copy-start | bytes 100
  105.5 50.6 %copy-start.22 = (s32[8]{0:T(128)S(1)}, s32[8]{0:T(128)}, u32[]{:S(2)}) copy-start(s32[8]{0:T(128)} %constant.71.clone) | copy-start | bytes 100
  105.5 52.5 %copy-start.21 = (s32[8]{0:T(128)S(1)}, s32[8]{0:T(128)}, u32[]{:S(2)}) copy-start(s32[8]{0:T(128)} %constant.72.clone) | copy-start | bytes 100
  105.5 54.4 %copy-start.20 = (s32[8]{0:T(128)S(1)}, s32[8]{0:T(128)}, u32[]{:S(2)}) copy-start(s32[8]{0:T(128)} %constant.73.clone) | copy-start | bytes 100
  105.5 56.0 %copy-start.19 = (s32[8]{0:T(128)S(1)}, s32[8]{0:T(128)}, u32[]{:S(2)}) copy-start(s32[8]{0:T(128)} %constant.74.clone) | copy-start | bytes 100
  105.5 57.9 %copy-start.18 = (s32[8]{0:T(128)S(1)}, s32[8]{0:T(128)}, u32[]{:S(2)}) copy-start(s32[8]{0:T(128)} %constant.75.clone) | copy-start | bytes 100
  105.6 59.7 %copy-start.17 = (s32[8]{0:T(128)S(1)}, s32[8]{0:T(128)}, u32[]{:S(2)}) copy-start(s32[8]{0:T(128)} %constant.76.clone) | copy-start | bytes 100
  105.6 61.5 %copy-start.11 = (bf16[512]{0:T(512)(128)(2,1)S(1)}, bf16[512]{0:T(512)(128)(2,1)}, u32[]{:S(2)}) copy-start(bf16[512]{0:T(512)(128)(2,1)} %param.35) | copy-start | bytes 3076
  105.6 61.5 %copy-start.12 = (bf16[512]{0:T(512)(128)(2,1)S(1)}, bf16[512]{0:T(512)(128)(2,1)}, u32[]{:S(2)}) copy-start(bf16[512]{0:T(512)(128)(2,1)} %param.34) | copy-start | bytes 3076
  105.6 65.8 %copy-start.9 = (bf16[3,1408]{1,0:T(4,128)(2,1)S(1)}, bf16[3,1408]{1,0:T(4,128)(2,1)}, u32[]{:S(2)}) copy-start(bf16[3,1408]{1,0:T(4,128)(2,1)} %param.38) | copy-start | bytes 25348
  105.6 65.8 %copy-start.10 = (bf16[3,1408]{1,0:T(4,128)(2,1)S(1)}, bf16[3,1408]{1,0:T(4,128)(2,1)}, u32[]{:S(2)}) copy-start(bf16[3,1408]{1,0:T(4,128)(2,1)} %param.39) | copy-start | bytes 25348
  105.6 85.9 %all-to-all-start = ((bf16[4,384,512]{2,1,0:T(8,128)(2,1)}), bf16[4,384,512]{2,1,0:T(8,128)(2,1)S(1)}, u32[]{:S(2)}, u32[]{:S(2)}) async-start(bf16[4,384,512]{2,1,0:T(8,128)(2,1)} %pad_maximum_fusion), calls=%async_computation | async-start | bytes 3145728 | tf_op jit(solution)/shard_map/all_to_all | solution.py:122
  111.0 74.5 %collective-permute-start.10 = (bf16[1408,256]{1,0:T(8,128)(2,1)}, bf16[1408,256]{1,0:T(8,128)(2,1)}, u32[]{:S(2)}, u32[]{:S(2)}) collective-permute-start(bf16[1408,256]{1,0:T(8,128)(2,1)} %param.40), channel_id=1, source_target_pairs={{0,4},{8,0},{16,8},{24,16},{28,24},{20,28},{12,20},{4,12},{1,5},{9... | collective-permute-start | bytes 2162696 | tf_op jit(solution)/shard_map/ppermute | solution.py:60
  111.0 78.4 %collective-permute-start.7 = (bf16[1408,256]{1,0:T(8,128)(2,1)}, bf16[1408,256]{1,0:T(8,128)(2,1)}, u32[]{:S(2)}, u32[]{:S(2)}) collective-permute-start(bf16[1408,256]{1,0:T(8,128)(2,1)} %collective-permute-done.6), channel_id=1, source_target_pairs={{0,8},{8,16},{16,24},{24,28},{28,20},{20,12},{12,4},{4,0},{1,9},{9... | collective-permute-start | bytes 2162696 | tf_op jit(solution)/shard_map/ppermute | solution.py:60
  152.3 33.1 %collective-permute-start.4 = (s32[2]{0:T(128)S(1)}, s32[2]{0:T(128)S(1)}, u32[]{:S(2)}, u32[]{:S(2)}) collective-permute-start(s32[2]{0:T(128)S(1)} %slice.110), channel_id=1, source_target_pairs={{0,4},{4,8},{8,12},{12,16},{16,20},{20,24},{24,28},{1,5},{5,9},{9,... | collective-permute-start | bytes 32 | tf_op jit(solution)/shard_map/ppermute | solution.py:27
  185.5 80.0 %collective-permute-start.11 = (bf16[1408,256]{1,0:T(8,128)(2,1)}, bf16[1408,256]{1,0:T(8,128)(2,1)}, u32[]{:S(2)}, u32[]{:S(2)}) collective-permute-start(bf16[1408,256]{1,0:T(8,128)(2,1)} %collective-permute-done.10), channel_id=1, source_target_pairs={{0,4},{8,0},{16,8},{24,16},{28,24},{20,28},{12,20},{4,12},{1,5},{9... | collective-permute-start | bytes 2162696 | tf_op jit(solution)/shard_map/ppermute | solution.py:60
  189.4 76.1 %collective-permute-start.8 = (bf16[1408,256]{1,0:T(8,128)(2,1)}, bf16[1408,256]{1,0:T(8,128)(2,1)}, u32[]{:S(2)}, u32[]{:S(2)}) collective-permute-start(bf16[1408,256]{1,0:T(8,128)(2,1)} %collective-permute-done.7), channel_id=1, source_target_pairs={{0,8},{8,16},{16,24},{24,28},{28,20},{20,12},{12,4},{4,0},{1,9},{9... | collective-permute-start | bytes 2162696 | tf_op jit(solution)/shard_map/ppermute | solution.py:60
  200.1 19.1 %copy-start.3 = (bf16[384,512]{1,0:T(8,128)(2,1)}, bf16[384,512]{1,0:T(8,128)(2,1)S(1)}, u32[]{:S(2)}) copy-start(bf16[384,512]{1,0:T(8,128)(2,1)S(1)} %add_convert_fusion.1) | copy-start | bytes 1179652
  225.9 41.0 %collective-permute-start.5 = (bf16[2,1408]{1,0:T(2,128)(2,1)S(1)}, bf16[2,1408]{1,0:T(2,128)(2,1)S(1)}, u32[]{:S(2)}, u32[]{:S(2)}) collective-permute-start(bf16[2,1408]{1,0:T(2,128)(2,1)S(1)} %slice.138), channel_id=1, source_target_pairs={{0,4},{4,8},{8,12},{12,16},{16,20},{20,24},{24,28},{1,5},{5,9},{9,... | collective-permute-start | bytes 16904 | tf_op jit(solution)/shard_map/ppermute | solution.py:27
  259.9 7.1 %collective-permute-start.3 = (bf16[2,1408]{1,0:T(2,128)(2,1)S(1)}, bf16[2,1408]{1,0:T(2,128)(2,1)S(1)}, u32[]{:S(2)}, u32[]{:S(2)}) collective-permute-start(bf16[2,1408]{1,0:T(2,128)(2,1)S(1)} %slice.135), channel_id=1, source_target_pairs={{0,4},{4,8},{8,12},{12,16},{16,20},{20,24},{24,28},{1,5},{5,9},{9,... | collective-permute-start | bytes 16904 | tf_op jit(solution)/shard_map/ppermute | solution.py:27
  265.5 20.3 %collective-permute-start.12 = (bf16[1408,256]{1,0:T(8,128)(2,1)}, bf16[1408,256]{1,0:T(8,128)(2,1)S(1)}, u32[]{:S(2)}, u32[]{:S(2)}) collective-permute-start(bf16[1408,256]{1,0:T(8,128)(2,1)} %collective-permute-done.11), channel_id=1, source_target_pairs={{0,4},{8,0},{16,8},{24,16},{28,24},{20,28},{12,20},{4,12},{1,5},{9... | collective-permute-start | bytes 2162696 | tf_op jit(solution)/shard_map/ppermute | solution.py:60
  265.5 16.6 %collective-permute-start.9 = (bf16[1408,256]{1,0:T(8,128)(2,1)}, bf16[1408,256]{1,0:T(8,128)(2,1)S(1)}, u32[]{:S(2)}, u32[]{:S(2)}) collective-permute-start(bf16[1408,256]{1,0:T(8,128)(2,1)} %collective-permute-done.8), channel_id=1, source_target_pairs={{0,8},{8,16},{16,24},{24,28},{28,20},{20,12},{12,4},{4,0},{1,9},{9... | collective-permute-start | bytes 2162696 | tf_op jit(solution)/shard_map/ppermute | solution.py:60
  286.2 1.2 copy-start.2
  287.4 6.1 %copy-start.13 = (bf16[512]{0:T(512)(128)(2,1)S(1)}, bf16[512]{0:T(512)(128)(2,1)}, u32[]{:S(2)}) copy-start(bf16[512]{0:T(512)(128)(2,1)} %param.42) | copy-start | bytes 3076
  287.4 6.1 %copy-start.14 = (bf16[512]{0:T(512)(128)(2,1)S(1)}, bf16[512]{0:T(512)(128)(2,1)}, u32[]{:S(2)}) copy-start(bf16[512]{0:T(512)(128)(2,1)} %param.41) | copy-start | bytes 3076
  287.4 24.3 %all-to-all-start.1 = ((bf16[4,2,384,256]{3,2,1,0:T(8,128)(2,1)}), bf16[4,2,384,256]{3,2,1,0:T(8,128)(2,1)S(1)}, u32[]{:S(2)}, u32[]{:S(2)}) async-start(bf16[4,2,384,256]{3,2,1,0:T(8,128)(2,1)} %bitcast.79), calls=%async_computation.1 | async-start | bytes 3145728 | tf_op jit(solution)/shard_map/all_to_all | solution.py:261
  293.4 18.5 %copy-start.4 = (bf16[384,512]{1,0:T(8,128)(2,1)S(1)}, bf16[384,512]{1,0:T(8,128)(2,1)}, u32[]{:S(2)}) copy-start(bf16[384,512]{1,0:T(8,128)(2,1)} %copy-done.3) | copy-start | bytes 1179652
Sparse Core Ops, SparseCore 0:
  9.5 127.4 all-gather.4
  139.2 114.9 all-gather.2
where the time goes:
time: 330 us; the launch traced here: 326 us
  waiting for transfers between devices  113 us (34%)
  starting transfers between devices  74 us (22%)
  blocking collectives  29.5 us (9%)
  matrix products  27.3 us (8%)
  between operations  26.9 us (8%)
  other arithmetic  24.5 us (7%)
  Pallas kernels  17.2 us (5%)
  local copies, waits for them, and re-layouts  13.7 us (4%)
    ppermute x6, waiting for transfers between devices, passed_along(): return lax.ppermute(value, axis, pairs)  57.3 us
    ppermute x7, starting transfers between devices, ring_blocks(): moving = lax.ppermute(moving, axis, pairs)  45 us
    all_gather x1, waiting for transfers between devices, local(): whole_value = lax.all_gather(ffn_value, 'sp', axis=0, tiled=True)  26.3 us
    all_to_all x1, waiting for transfers between devices, local(): lax.all_to_all(unit_terms.reshape(tp_count, share, row_count, block_width...  18.2 us
    ppermute x6, starting transfers between devices, passed_along(): return lax.ppermute(value, axis, pairs)  17.5 us
    pallas_call x1, Pallas kernels, attend(): pl.pallas_call(functools.partial(attend_kernel, chunk, window - rows, sca...  17.2 us
    dot_general x8, matrix products, local(): jnp.dot(hidden, block, preferred_element_type=jnp.float32)  10.5 us
    all_gather x1, blocking collectives, local(): lax.all_gather(normed[:half], 'tp', axis=1, tiled=True)  9.35 us
  transfers between devices with their start and end apart: 17, of which 8 were waited for; matrix products, arithmetic and copies ran while one was open for 19% of the time, Pallas kernels for 5%

commit v1 on v0

--- a/solution.py
+++ b/solution.py
@@ -131,7 +131,7 @@
     ) * gain_row.astype(jnp.float32) + bias_row.astype(jnp.float32)
 
 
-def local(
+def plain(
     residual,
     query_nope,
     query_rope,
@@ -268,6 +268,637 @@
     return finish(mixed_two, totals_two, norm2_gain, norm2_bias).astype(jnp.bfloat16)
 
 
+LANES = 128
+MESH = pl.DeviceIdType.MESH
+log2_e = 1.4426950408889634
+
+
+class Copies:
+    def __init__(self, send_sems, recv_sems):
+        self.send_sems, self.recv_sems = send_sems, recv_sems
+        self.count = 0
+
+    def ids(self, number=1):
+        first = self.count
+        self.count += number
+        return first
+
+    def make(self, index, source, target, sp, tp):
+        return pltpu.make_async_remote_copy(
+            src_ref=source,
+            dst_ref=target,
+            send_sem=self.send_sems.at[index],
+            recv_sem=self.recv_sems.at[index],
+            device_id={"sp": sp, "tp": tp},
+            device_id_type=MESH,
+        )
+
+
+REMOTE = 160
+LOCAL = 16
+
+
+def flip(value, bits):
+    for bit in range(bits.bit_length()):
+        step = 1 << bit
+        if bits & step:
+            value = value + step - 2 * step * ((value // step) % 2)
+    return value
+
+
+def layer_kernel(
+    sizes,
+    q_in, t_in, pack_in, kup_in, vup_in, proj_in, resid_in, gains, taps, gate_in, value_in, down_in,
+    out_ref,
+    win, q_v, t_v, kup, vup, proj, resid, keys, vals, ropes, bias, att,
+    core_out, core_in, keep, y_out, y_in, mix, stat_own, stat_in, valid,
+    rows_all, gate_w, value_w, down_w, ext, hid,
+    core_out2, core_in2, keep2, y_out2, y_in2, z_out2, z_in2, stat_own2, stat_in2,
+    send_sems, recv_sems, local_sems,
+):
+    n_sp, n_tp, R, reach, heads, wide, first, second = sizes
+    C = LANES
+    F = resid.shape[1]
+    chunks = R // C
+    window = (reach + 1) * R
+    span = C + reach * R
+    latent_width = kup.shape[0]
+    gate_rows = gate_in.shape[0]
+    down_cols = down_in.shape[1]
+    bf16, f32 = jnp.bfloat16, jnp.float32
+    me_sp, me_tp = lax.axis_index("sp"), lax.axis_index("tp")
+    x, z = me_sp % 2, me_sp // 2
+    odd = z % 2
+    y, c = me_tp // 2, me_tp % 2
+    x_peer = me_sp + 1 - 2 * x
+    c_peer = me_tp + 1 - 2 * c
+    y_peer = me_tp + 2 - 4 * y
+    far_peer = 3 - me_tp
+    nz = n_sp // 2
+    z_sp = [2 * flip(z, d) + x for d in range(nz)]
+    pair = z_sp[1]
+    rc = Copies(send_sems, recv_sems)
+    sent = []
+
+    def start(copy, when=None):
+        if when is None:
+            copy.start()
+        else:
+            pl.when(when)(copy.start)
+        sent.append((copy, when))
+
+    barrier = pltpu.get_barrier_semaphore()
+    for i in range(n_sp):
+        for j in range(n_tp):
+            if i or j:
+                pl.semaphore_signal(
+                    barrier, inc=1,
+                    device_id={"sp": (me_sp + i) % n_sp, "tp": (me_tp + j) % n_tp},
+                    device_id_type=MESH,
+                )
+
+    loads = {}
+
+    def load(name, source, target):
+        loads[name] = pltpu.make_async_copy(source, target, local_sems.at[len(loads)])
+        loads[name].start()
+
+    load("win", pack_in, win.at[pl.ds(reach * R, R)])
+    load("kup", kup_in, kup)
+    load("vup", vup_in, vup)
+    load("q", q_in, q_v)
+    load("t", t_in, t_v)
+    load("proj", proj_in, proj)
+    load("resid", resid_in, resid)
+
+    pl.semaphore_wait(barrier, n_sp * n_tp - 1)
+
+    half = R // 2
+    halo, halo_core = rc.ids(reach), rc.ids(reach)
+
+    def halo_copy(k):
+        return rc.make(
+            halo + k - 1,
+            pack_in.at[pl.ds(c * half, half)],
+            win.at[pl.ds((reach - k) * R + c * half, half)],
+            me_sp + k, me_tp,
+        )
+
+    def halo_pass(k, core):
+        rows = win.at[pl.ds((reach - k) * R + core * half, half)]
+        return rc.make(halo_core + k - 1, rows, rows, me_sp, c_peer)
+
+    for k in range(1, reach + 1):
+        start(halo_copy(k), me_sp + k < n_sp)
+
+    halves = ((0, first), (first, second))
+
+    def half_in(w, parity):
+        at, size = halves[parity]
+        if w == 2:
+            return down_in.at[pl.ds(at, size), :]
+        return (gate_in, value_in)[w].at[:, pl.ds(at, size)]
+
+    def half_slot(w, parity, owner):
+        size = halves[parity][1]
+        if w == 2:
+            return down_w.at[owner, pl.ds(0, size), :]
+        rows = pl.ds(pl.multiple_of(owner * gate_rows, 16), gate_rows)
+        return (gate_w, value_w)[w].at[rows, pl.ds(0, size)]
+
+    def by_parity(parity, act):
+        for p in range(2):
+            pl.when(parity == p)(functools.partial(act, p))
+
+    z_ids = [rc.ids(nz) for _ in range(3)]
+    x_ids = [rc.ids(nz) for _ in range(3)]
+    own_ids = [len(loads) + w for w in range(3)]
+
+    def own_weight(w, p):
+        return pltpu.make_async_copy(half_in(w, p), half_slot(w, p, me_sp), local_sems.at[own_ids[w]])
+
+    def z_weight(w, d, p):
+        return rc.make(z_ids[w] + d, half_in(w, p), half_slot(w, p, me_sp), z_sp[d], me_tp)
+
+    def z_landed(w, d, p):
+        return rc.make(z_ids[w] + d, half_in(w, p), half_slot(w, p, z_sp[d]), z_sp[d], me_tp)
+
+    def x_weight(w, d, p):
+        source = half_in(w, p) if d == 0 else half_slot(w, p, z_sp[d])
+        return rc.make(x_ids[w] + d, source, half_slot(w, p, z_sp[d]), x_peer, me_tp)
+
+    def x_landed(w, d, p):
+        slot = half_slot(w, p, z_sp[d] + 1 - 2 * x)
+        return rc.make(x_ids[w] + d, slot, slot, x_peer, me_tp)
+
+    def send_z(w):
+        for d in list(range(2, nz)) + [1]:
+            by_parity((odd + d) % 2, lambda p, d=d: z_weight(w, d, p).start())
+
+    def send_x(w, d):
+        if d:
+            by_parity(odd, lambda p: z_landed(w, d, p).wait_recv())
+        by_parity(odd, lambda p: x_weight(w, d, p).start())
+
+    def all_here(w):
+        def act(p):
+            own_weight(w, p).wait()
+            for d in range(nz):
+                x_landed(w, d, p).wait_recv()
+        by_parity(odd, act)
+
+    for w in range(3):
+        by_parity(odd, lambda p, w=w: own_weight(w, p).start())
+    send_x(0, 0)
+    send_z(0)
+    send_x(1, 0)
+
+    @pl.when(odd == 1)
+    def _():
+        blank = first - second
+        if blank:
+            gate_w[:, second:] = jnp.zeros((gate_w.shape[0], blank), bf16)
+            value_w[:, second:] = jnp.zeros((gate_w.shape[0], blank), bf16)
+            down_w[:, second:, :] = jnp.zeros((n_sp, blank, down_cols), bf16)
+
+    loads["win"].wait()
+    loads["kup"].wait()
+    loads["vup"].wait()
+
+    def raise_rows(block):
+        rows = pl.ds(pl.multiple_of(block * R, LANES), R)
+        source = win[rows, :latent_width]
+        keys[rows, :] = jnp.dot(source, kup[...], preferred_element_type=f32).astype(bf16)
+        vals[rows, :] = jnp.dot(source, vup[...], preferred_element_type=f32).astype(bf16)
+
+    raise_rows(reach)
+    for k in range(1, reach + 1):
+        @pl.when(me_sp >= k)
+        def _(k=k):
+            halo_copy(k).wait_recv()
+            halo_pass(k, c).start()
+
+        @pl.when(me_sp < k)
+        def _(k=k):
+            win[(reach - k) * R : (reach - k + 1) * R, :] = jnp.zeros((R, win.shape[1]), bf16)
+        sent.append((halo_pass(k, c), me_sp >= k))
+    for k in range(1, reach + 1):
+        @pl.when(me_sp >= k)
+        def _(k=k):
+            halo_pass(k, 1 - c).wait_recv()
+
+    @pl.loop(0, reach)
+    def _(block):
+        raise_rows(block)
+
+    side = win[:, latent_width:]
+    side_f = side.astype(f32)
+    lane = lax.broadcasted_iota(jnp.int32, (window, LANES), 1)
+    low = lane < LANES // 2
+    ropes[0] = jnp.where(low, side_f, 0.0).astype(bf16)
+    ropes[1] = jnp.where(low, 0.0, pltpu.roll(side_f, LANES // 2, 1)).astype(bf16)
+    pick = (
+        (lax.broadcasted_iota(jnp.int32, (8, LANES), 1) == LANES // 2)
+        .astype(f32)
+        .astype(bf16)
+    )
+    key_doc = lax.dot_general(pick, side, (((1,), (1,)), ((), ())), preferred_element_type=f32)[0:1]
+    for r in range(chunks):
+        at = slice(r * C, (r + 1) * C)
+        own_doc = side_f[reach * R + r * C : reach * R + (r + 1) * C, LANES // 2 : LANES // 2 + 1]
+        key_at = lax.broadcasted_iota(jnp.int32, (C, window), 1) - reach * R
+        row_at = lax.broadcasted_iota(jnp.int32, (C, window), 0) + r * C
+        allowed = (key_at <= row_at) & (key_at + me_sp * R >= 0) & (key_doc == own_doc)
+        bias[at, :] = jnp.where(allowed, 0.0, masked_score)
+
+    tail = side_f[reach * R - 8 :]
+    valid_id = rc.ids()
+    row_no = lax.broadcasted_iota(jnp.int32, (R, LANES), 0) + me_sp * R
+    here = tail[8:]
+    back_one = (pltpu.roll(tail, 1, 0)[8:] == here) & (row_no >= 1)
+    back_two = (pltpu.roll(tail, 2, 0)[8:] == here) & (row_no >= 2)
+    lanes = lax.broadcasted_iota(jnp.int32, (R, LANES), 1)
+    valid[odd] = jnp.where(
+        lanes < 3 * LANES // 4, back_two.astype(f32), back_one.astype(f32)
+    ).astype(bf16)
+    start(rc.make(valid_id, valid.at[odd], valid.at[odd], pair, me_tp))
+
+    scale = (NOPE + ROPE) ** (-0.5) * log2_e
+
+    def attend_chunk(r):
+        at, seen = slice(r * C, (r + 1) * C), slice(r * C, r * C + span)
+
+        @pl.loop(0, heads // 2)
+        def _(duo):
+            turned = t_v[at, pl.ds(pl.multiple_of(duo * LANES, LANES), LANES)]
+            for e in range(2):
+                head = pl.ds(pl.multiple_of((2 * duo + e) * LANES, LANES), LANES)
+                queries = jnp.concatenate([q_v[at, head], turned], 1)
+                seen_keys = jnp.concatenate([keys[seen, head], ropes[e, seen, :]], 1)
+                scores = lax.dot_general(
+                    queries, seen_keys, (((1,), (1,)), ((), ())), preferred_element_type=f32
+                )
+                scores = scores * scale + bias[at, seen]
+                weights = jnp.exp2(scores - jnp.max(scores, -1, keepdims=True))
+                total = jnp.sum(weights, -1, keepdims=True)
+                mixed = jnp.dot(weights.astype(bf16), vals[seen, head], preferred_element_type=f32)
+                att[at, head] = (mixed * (1.0 / total)).astype(bf16)
+
+    core_ids, y_ids = rc.ids(2 * chunks), rc.ids(chunks)
+    stat_ids = rc.ids(3 * chunks)
+    stat_ids2 = rc.ids(3 * chunks)
+    gather_ids = rc.ids(8 * chunks)
+
+    def to_core(r, i):
+        return rc.make(core_ids + 2 * r + i, core_out.at[r, i], core_in.at[r, i], me_sp, c_peer)
+
+    def to_y(r):
+        return rc.make(y_ids + r, y_out.at[r], y_in.at[r], me_sp, y_peer)
+
+    def features(tp):
+        return pl.ds(pl.multiple_of(tp * F, LANES), F)
+
+    def project(r):
+        rows = att[r * C : (r + 1) * C, :]
+        for i, yy in enumerate((1 - y, y)):
+            core_out[r, i] = jnp.dot(
+                rows, proj[:, features(2 * yy + 1 - c)], preferred_element_type=f32
+            ).astype(bf16)
+            start(to_core(r, i))
+        for i, yy in enumerate((1 - y, y)):
+            keep[r, i] = jnp.dot(
+                rows, proj[:, features(2 * yy + c)], preferred_element_type=f32
+            ).astype(bf16)
+        to_core(r, 0).wait_recv()
+        y_out[r] = (keep[r, 0].astype(f32) + core_in[r, 0].astype(f32)).astype(bf16)
+        start(to_y(r))
+
+    def stat_copy(ids, own, landed, r, i):
+        return rc.make(ids + 3 * r + i, own.at[r], landed.at[r, i], me_sp, (c_peer, y_peer, far_peer)[i])
+
+    def send_stats(values, ids, own, landed, r):
+        one = jnp.sum(values, -1, keepdims=True)
+        two = jnp.sum(values * values, -1, keepdims=True)
+        lane = lax.broadcasted_iota(jnp.int32, (C, LANES), 1)
+        own[r] = jnp.where(lane % 8 < 4, one, two).T[0:8]
+        for i in (1, 2, 0):
+            start(stat_copy(ids, own, landed, r, i))
+
+    def norm(values, ids, own, landed, r, gain):
+        for i in range(3):
+            stat_copy(ids, own, landed, r, i).wait_recv()
+        total = (own[r] + landed[r, 0]) + (landed[r, 1] + landed[r, 2])
+        total = jnp.concatenate([total] * (LANES // 8), 0).T
+        row_mean = total[:, 0:1] / wide
+        row_power = total[:, 4:5] / wide
+        return (values - row_mean) * lax.rsqrt(row_power - row_mean * row_mean + norm_eps) * gains[
+            gain : gain + 1, :
+        ] + gains[gain + 1 : gain + 2, :]
+
+    def mix_one(r):
+        at = slice(r * C, (r + 1) * C)
+        to_core(r, 1).wait_recv()
+        to_y(r).wait_recv()
+        mixed = residual_scale * resid[at, :].astype(f32) + (
+            keep[r, 1].astype(f32) + core_in[r, 1].astype(f32) + y_in[r].astype(f32)
+        )
+        mix[at, :] = mixed
+        send_stats(mixed, stat_ids, stat_own, stat_in, r)
+
+    def gathered(r, kind, slot, tp, sp_to, tp_to):
+        spot = rows_all.at[slot, pl.ds(r * C, C), features(tp)]
+        return rc.make(gather_ids + 8 * r + kind, spot, spot, sp_to, tp_to)
+
+    def to_pair(r, slot):
+        return gathered(r, 0, slot, me_tp, pair, me_tp)
+
+    def core_gather(r, kind, slot, tp):
+        return gathered(r, kind, slot, tp, me_sp, c_peer)
+
+    def y_gather(r, kind, slot, tp):
+        return gathered(r, kind, slot, tp, me_sp, y_peer)
+
+    def norm_one(r):
+        at = slice(r * C, (r + 1) * C)
+        rows_all[odd, at, features(me_tp)] = norm(
+            mix[at, :], stat_ids, stat_own, stat_in, r, 0
+        ).astype(bf16)
+        start(to_pair(r, odd))
+        start(y_gather(r, 1, odd, me_tp))
+        start(core_gather(r, 2, odd, me_tp))
+
+    def pass_pair(r):
+        to_pair(r, 1 - odd).wait_recv()
+        start(y_gather(r, 3, 1 - odd, me_tp))
+        start(core_gather(r, 4, 1 - odd, me_tp))
+
+    def pass_y(r):
+        for kind, got, slot in ((5, 1, odd), (6, 3, 1 - odd)):
+            y_gather(r, got, slot, y_peer).wait_recv()
+            start(core_gather(r, kind, slot, y_peer))
+
+    def rows_here(r):
+        core_gather(r, 2, odd, c_peer).wait_recv()
+        core_gather(r, 4, 1 - odd, c_peer).wait_recv()
+        core_gather(r, 5, odd, far_peer).wait_recv()
+        core_gather(r, 6, 1 - odd, far_peer).wait_recv()
+
+    loads["q"].wait()
+    loads["t"].wait()
+    attend_chunk(0)
+    loads["proj"].wait()
+    loads["resid"].wait()
+    project(0)
+    for r in range(1, chunks):
+        attend_chunk(r)
+        mix_one(r - 1)
+        project(r)
+        norm_one(r - 1)
+    mix_one(chunks - 1)
+    norm_one(chunks - 1)
+    for d in range(1, nz):
+        send_x(0, d)
+    send_z(1)
+    send_z(2)
+    send_x(2, 0)
+    for r in range(chunks):
+        pass_pair(r)
+    for r in range(chunks):
+        pass_y(r)
+    for r in range(chunks):
+        rows_here(r)
+
+    tile = 2 * LANES
+    mid = first
+
+    def up(weights, base):
+        @pl.loop(0, 2)
+        def _(slot):
+            @pl.loop(0, first // tile)
+            def _(j):
+                cols = pl.multiple_of(j * tile, LANES)
+                ext[slot, 8:, pl.ds(base + cols, tile)] = (
+                    jnp.dot(rows_all[slot], weights[:, pl.ds(cols, tile)], preferred_element_type=f32)
+                    .astype(bf16)
+                    .astype(f32)
+                )
+
+    all_here(0)
+    up(gate_w, 0)
+    for d in range(1, nz):
+        send_x(1, d)
+    all_here(1)
+    up(value_w, mid)
+
+    tail_ids = rc.ids(2)
+
+    def tail_copy(slot, to_slot, sp):
+        return rc.make(
+            tail_ids + to_slot, ext.at[slot, pl.ds(R, 8)], ext.at[to_slot, pl.ds(0, 8)], sp, me_tp
+        )
+
+    last_pair = z >= nz - 2
+    start(tail_copy(0, 0, x_peer), x == 0)
+    start(tail_copy(1, 1, x_peer), x == 0)
+    start(tail_copy(0, 1, x_peer), x == 1)
+    start(tail_copy(1, 0, me_sp + 3), (x == 1) & (z < nz - 2))
+
+    @pl.when((x == 0) & (z < 2))
+    def _():
+        ext[0, 0:8, :] = jnp.zeros((8, ext.shape[2]), f32)
+
+    for d in range(1, nz):
+        send_x(2, d)
+
+    @pl.when((x == 1) | (z >= 2))
+    def _():
+        tail_copy(0, 0, x_peer).wait_recv()
+    tail_copy(1, 1, x_peer).wait_recv()
+    rc.make(valid_id, valid.at[1 - odd], valid.at[1 - odd], pair, me_tp).wait_recv()
+
+    deep = 64
+
+    @pl.loop(0, 2)
+    def _(slot):
+        @pl.loop(0, R // deep)
+        def _(i):
+            at = pl.multiple_of(i * deep, 16)
+            marks = valid[slot, pl.ds(at, deep), :].astype(f32)
+            two, one = marks[:, LANES // 2 : LANES // 2 + 1], marks[:, LANES - 1 : LANES]
+
+            @pl.loop(0, first // tile)
+            def _(j):
+                cols = pl.multiple_of(j * tile, LANES)
+
+                def mixing(base, tap):
+                    rows = ext[slot, pl.ds(at, deep + 8), pl.ds(base + cols, tile)]
+                    weight = taps[pl.ds(tap, 8), pl.ds(cols, tile)]
+                    return (
+                        weight[0:1] * (pltpu.roll(rows, 2, 0)[8:] * two)
+                        + weight[1:2] * (pltpu.roll(rows, 1, 0)[8:] * one)
+                        + weight[2:3] * rows[8:]
+                    )
+
+                hid[slot, pl.ds(at, deep), pl.ds(cols, tile)] = (
+                    mixing(mid, 8) * jax.nn.gelu(mixing(0, 0))
+                ).astype(bf16)
+
+    all_here(2)
+
+    core_ids2, y_ids2, z_id2 = rc.ids(4), rc.ids(2), rc.ids()
+    per = F // down_cols
+
+    def down(slot, tp, target):
+        for j in range(per):
+            target[:, j * down_cols : (j + 1) * down_cols] = jnp.dot(
+                hid[slot], down_w[per * tp + j], preferred_element_type=f32
+            ).astype(bf16)
+
+    def to_core2(i, s):
+        return rc.make(
+            core_ids2 + 2 * i + s, core_out2.at[i, s], core_in2.at[i, s], me_sp, c_peer
+        )
+
+    def to_y2(s):
+        return rc.make(y_ids2 + s, y_out2.at[s], y_in2.at[s], me_sp, y_peer)
+
+    slots = (1 - odd, odd)
+    for i, yy in enumerate((1 - y, y)):
+        for s, slot in enumerate(slots):
+            down(slot, 2 * yy + 1 - c, core_out2.at[i, s])
+            start(to_core2(i, s))
+            down(slot, 2 * yy + c, keep2.at[i, s])
+            to_core2(i, s).wait_recv()
+            if i == 0:
+                y_out2[s] = (keep2[0, s].astype(f32) + core_in2[0, s].astype(f32)).astype(bf16)
+                start(to_y2(s))
+    to_y2(0).wait_recv()
+    z_out2[...] = (
+        keep2[1, 0].astype(f32) + core_in2[1, 0].astype(f32) + y_in2[0].astype(f32)
+    ).astype(bf16)
+    to_z2 = rc.make(z_id2, z_out2, z_in2, pair, me_tp)
+    start(to_z2)
+    to_y2(1).wait_recv()
+    to_z2.wait_recv()
+    for r in range(chunks):
+        at = slice(r * C, (r + 1) * C)
+        mixed = residual_scale * rows_all[odd, at, features(me_tp)].astype(f32) + (
+            keep2[1, 1, at, :].astype(f32)
+            + core_in2[1, 1, at, :].astype(f32)
+            + y_in2[1, at, :].astype(f32)
+            + z_in2[at, :].astype(f32)
+        )
+        mix[at, :] = mixed
+        send_stats(mixed, stat_ids2, stat_own2, stat_in2, r)
+    for r in range(chunks):
+        at = slice(r * C, (r + 1) * C)
+        out_ref[at, :] = norm(mix[at, :], stat_ids2, stat_own2, stat_in2, r, 2).astype(bf16)
+
+    for copy, when in sent:
+        if when is None:
+            copy.wait_send()
+        else:
+            pl.when(when)(copy.wait_send)
+    for w in range(3):
+        for d in range(nz):
+            if d:
+                by_parity((odd + d) % 2, lambda p, d=d, w=w: z_weight(w, d, p).wait_send())
+            by_parity(odd, lambda p, d=d, w=w: x_weight(w, d, p).wait_send())
+    assert rc.count <= REMOTE, rc.count
+
+
+def fused(
+    residual, query_nope, query_rope, latent, rope_key, doc_ids, key_up, value_up, out_proj,
+    norm1_gain, norm1_bias, ffn_gate, ffn_value, conv_gate, conv_value, ffn_down, norm2_gain, norm2_bias,
+):
+    n_sp, n_tp = lax.axis_size("sp"), lax.axis_size("tp")
+    R, F = residual.shape
+    heads = query_nope.shape[1] // NOPE
+    units = ffn_gate.shape[1]
+    first = -(-units // (2 * LANES)) * LANES
+    second = units - first
+    window = (REACH + 1) * R
+    chunks = R // LANES
+    f32, bf16 = jnp.float32, jnp.bfloat16
+    offset = lax.axis_index("sp") * R
+    positions = offset + jnp.arange(R, dtype=jnp.int32)
+    half = ROPE // 2
+    place = jnp.arange(LANES, dtype=jnp.int32) % half
+    frequencies = 1.0 / rope_base_freq ** (2.0 * place.astype(f32) / ROPE)
+    angles = positions.astype(f32)[:, None] * frequencies[None, :]
+    cosine, sine = jnp.cos(angles), jnp.sin(angles)
+
+    def turn(vectors):
+        width = vectors.shape[1]
+        row = lax.broadcasted_iota(jnp.int32, (width, width), 0)
+        col = lax.broadcasted_iota(jnp.int32, (width, width), 1)
+        front = col % ROPE < half
+        swap = jnp.where(front & (row == col + half), -1.0, 0.0) + jnp.where(
+            ~front & (row == col - half), 1.0, 0.0
+        )
+        swapped = jnp.dot(vectors, swap.astype(bf16), preferred_element_type=f32)
+        times = max(1, width // LANES)
+        cos_wide = jnp.tile(cosine, (1, times))[:, :width]
+        sin_wide = jnp.tile(sine, (1, times))[:, :width]
+        return (vectors.astype(f32) * cos_wide + swapped * sin_wide).astype(bf16)
+
+    packed = jnp.concatenate(
+        [latent, turn(rope_key), jnp.broadcast_to(doc_ids.astype(bf16)[:, None], (R, ROPE))], 1
+    )
+    gains = jnp.stack([norm1_gain, norm1_bias, norm2_gain, norm2_bias]).astype(f32)
+    odd = (lax.axis_index("sp") // 2) % 2
+    blank = jnp.zeros((5, units), f32)
+    taps = jnp.concatenate([conv_gate.astype(f32), blank, conv_value.astype(f32), blank], 0)
+    taps = jnp.where(
+        odd == 0, taps[:, :first], jnp.pad(taps[:, first:], ((0, 0), (0, first - second)))
+    )
+    hbm = pl.BlockSpec(memory_space=pl.ANY)
+    vmem = pl.BlockSpec(memory_space=pltpu.VMEM)
+    sizes = (n_sp, n_tp, R, REACH, heads, n_tp * F, first, second)
+
+    def v(*shape, dtype=bf16):
+        return pltpu.VMEM(shape, dtype)
+
+    C = LANES
+    return pl.pallas_call(
+        functools.partial(layer_kernel, sizes),
+        in_specs=[hbm] * 7 + [vmem] * 2 + [hbm] * 3,
+        out_specs=vmem,
+        out_shape=jax.ShapeDtypeStruct((R, F), bf16),
+        scratch_shapes=[
+            v(window, packed.shape[1]), v(R, heads * NOPE), v(R, heads * ROPE),
+            v(*key_up.shape), v(*value_up.shape), v(*out_proj.shape), v(R, F),
+            v(window, heads * NOPE), v(window, heads * VDIM), v(2, window, LANES),
+            v(R, window, dtype=f32), v(R, heads * VDIM),
+            v(chunks, 2, C, F), v(chunks, 2, C, F), v(chunks, 2, C, F), v(chunks, C, F), v(chunks, C, F),
+            v(R, F, dtype=f32), v(chunks, 8, LANES, dtype=f32), v(chunks, 3, 8, LANES, dtype=f32),
+            v(2, R, LANES),
+            v(2, R, n_tp * F), v(n_sp * ffn_gate.shape[0], first), v(n_sp * ffn_gate.shape[0], first),
+            v(n_sp, first, ffn_down.shape[1]), v(2, R + 8, 2 * first, dtype=f32), v(2, R, first),
+            v(2, 2, R, F), v(2, 2, R, F), v(2, 2, R, F), v(2, R, F), v(2, R, F), v(R, F), v(R, F),
+            v(chunks, 8, LANES, dtype=f32), v(chunks, 3, 8, LANES, dtype=f32),
+            pltpu.SemaphoreType.DMA((REMOTE,)), pltpu.SemaphoreType.DMA((REMOTE,)),
+            pltpu.SemaphoreType.DMA((LOCAL,)),
+        ],
+        compiler_params=pltpu.CompilerParams(
+            collective_id=0, has_side_effects=True, vmem_limit_bytes=64 * 1024 * 1024 - 65536
+        ),
+    )(
+        query_nope, turn(query_rope), packed, key_up, value_up, out_proj, residual, gains, taps,
+        ffn_gate, ffn_value, ffn_down,
+    )
+
+
+def local(*arrays):
+    rows, features = arrays[0].shape
+    down_cols = arrays[15].shape[1]
+    n_sp, n_tp = lax.axis_size("sp"), lax.axis_size("tp")
+    paired = n_sp // 2
+    fits = n_tp == 4 and n_sp % 4 == 0 and paired & (paired - 1) == 0
+    tiled = rows % LANES == 0 and down_cols % LANES == 0 and features % down_cols == 0
+    return (fused if fits and tiled else plain)(*arrays)
+
+
 def solution(mesh):
     placed = (
         P("sp", "tp"),

time: 330 us -> 203 us (0.62)
  Pallas kernels: 17.2 us -> 192 us
  waiting for transfers between devices: 113 us -> 0 us
  starting transfers between devices: 74 us -> 0 us
  blocking collectives: 29.5 us -> 0 us
  between operations: 26.9 us -> 0.28 us
  matrix products: 27.3 us -> 2.81 us
  other arithmetic: 24.5 us -> 2.96 us
  local copies, waits for them, and re-layouts: 13.7 us -> 2.36 us
    pallas_call x1, Pallas kernels: 17.2 us -> 192 us  [fused(): pl.pallas_call(functools.partial(layer_kernel, sizes), in_specs=[hbm] * 7...]
    ppermute x13 -> x0, waiting for transfers between devices: 66.6 us -> none  [the longest x6 57.3 us: passed_along(): return lax.ppermute(value, axis, pairs)]
    ppermute x13 -> x0, starting transfers between devices: 62.5 us -> none  [the longest x7 45 us: ring_blocks(): moving = lax.ppermute(moving, axis, pairs)]
    all_gather x2 -> x0, waiting for transfers between devices: 26.3 us -> none  [the longest x1 26.3 us: local(): whole_value = lax.all_gather(ffn_value, 'sp', axis=0, tiled=True)]
    dot_general x13 -> x2, matrix products: 27.3 us -> 2.81 us  [turn(): swapped = jnp.dot(vectors, swap.astype(bf16), preferred_element_type=f32)]
    all_to_all x2 -> x0, waiting for transfers between devices: 18.2 us -> none  [the longest x1 18.2 us: local(): lax.all_to_all(unit_terms.reshape(tp_count, share, row_count, block_width...]
    all_gather x2 -> x0, blocking collectives: 18 us -> none  [the longest x1 9.35 us: local(): lax.all_gather(normed[:half], 'tp', axis=1, tiled=True)]
    psum x2 -> x0, blocking collectives: 11.5 us -> none  [the longest x1 5.85 us: local(): lax.psum((jnp.sum(mixed_one, 1), jnp.sum(mixed_one * mixed_one, 1)), 'tp')]
  transfers between devices with their start and end apart: 17 -> 0, of which waited for: 8 -> 0; matrix products, arithmetic and copies ran while one was open for 19% -> 0% of each run, Pallas kernels for 5% -> 0%
where the time goes in v1:
time: 203 us; the launch traced here: 201 us
  Pallas kernels  192 us (95%)
  other arithmetic  2.96 us (1%)
  matrix products  2.81 us (1%)
  local copies, waits for them, and re-layouts  2.36 us (1%)
    pallas_call x1, Pallas kernels, fused(): pl.pallas_call(functools.partial(layer_kernel, sizes), in_specs=[hbm] * 7...  192 us

profile of v1, /device:TPU:21, one launch (start us, length us, event | category | flops | bytes accessed | tf_op | source)
XLA Modules:
  0.0 200.6 jit_solution(4763564557479652814)
XLA Ops:
  0.0 0.0 copy-start.4
  0.0 0.0 copy-start.1
  0.0 0.0 copy-start
  0.0 0.8 multiply_cosine_fusion
  0.8 0.1 tile.20
  0.9 0.0 copy-start.5
  1.0 0.0 copy-start.6
  1.0 0.0 copy-start.7
  1.0 0.0 copy-start.8
  1.0 0.0 copy-start.2
  1.0 0.0 copy-start.3
  1.0 0.1 tile.8
  1.2 2.6 %fusion.2.t_in = bf16[384,512]{1,0:T(8,128)(2,1)} fusion(bf16[384,512]{1,0:T(8,128)(2,1)} %param.20, f32[48,8,4,128]{3,2,1,0:T(4,128)S(1)} %bitcast.26, f32[48,8,4,128]{3,2,1,0:T(4,128)S(1)} %bitcast.27, s32[512]{0:T(512)S(1)} %get-tuple-element.7, s32[512]{0:T(512)S(1)} %get-tuple-element.8, s32[512]{0:T(512)S(1)} %get-tuple-element.9, ...), kind=kOutput, calls=%fused_computation.5 | convolution fusion | flops 205193216 | bytes 2368000 | tf_op jit(solution)/shard_map/dot_general | solution.py:839
  3.8 0.0 copy-done.4
  3.8 0.1 broadcast_in_dim.41
  3.9 0.0 copy-done.1
  3.9 0.1 copy.20
  4.1 0.2 fusion.5
  4.3 0.0 copy-done
  4.3 0.9 pad_maximum_fusion.pack_in
  5.2 0.0 copy-done.5
  5.2 0.0 copy-done.6
  5.2 0.0 copy-done.7
  5.2 0.0 copy-done.8
  5.3 0.6 maximum_convert_fusion.gains
  5.9 0.0 copy-done.2
  5.9 0.0 copy-done.3
  6.0 0.6 fusion.18.taps
  6.6 192.2 %shard_map.172 = bf16[384,512]{1,0:T(8,128)(2,1)} custom-call(bf16[384,1024]{1,0:T(8,128)(2,1)} %q_in.1, bf16[384,512]{1,0:T(8,128)(2,1)} %fusion.2.t_in, bf16[384,640]{1,0:T(8,128)(2,1)} %pad_maximum_fusion.pack_in, bf16[512,1024]{1,0:T(8,128)(2,1)} %kup_in.1, bf16[512,1024]{1,0:T(8,128)(2,1)} %vup_in.1, bf16[1024,2048]{1,0:T(8,128)(2,1)} %proj_in.1, ...), custom_call_target="tpu_custom_call" | custom-call | tf_op jit(solution)/shard_map/pallas_call | solution.py:863
  198.9 1.8 copy.29
  (17 shorter events, 0.1 us)
Async XLA Ops:
  0.0 3.8 %copy-start.4 = (s32[384]{0:T(512)S(1)}, s32[384]{0:T(512)}, u32[]{:S(2)}) copy-start(s32[384]{0:T(512)} %param.23) | copy-start | bytes 4612
  0.0 3.9 %copy-start.1 = (bf16[384,64]{0,1:T(8,128)(2,1)S(1)}, bf16[384,64]{0,1:T(8,128)(2,1)}, u32[]{:S(2)}) copy-start(bf16[384,64]{0,1:T(8,128)(2,1)} %param.22) | copy-start | bytes 147460
  0.0 4.3 %copy-start = (bf16[384,512]{1,0:T(8,128)(2,1)S(1)}, bf16[384,512]{1,0:T(8,128)(2,1)}, u32[]{:S(2)}) copy-start(bf16[384,512]{1,0:T(8,128)(2,1)} %param.21) | copy-start | bytes 1179652
  0.9 4.3 %copy-start.5 = (bf16[512]{0:T(512)(128)(2,1)S(1)}, bf16[512]{0:T(512)(128)(2,1)}, u32[]{:S(2)}) copy-start(bf16[512]{0:T(512)(128)(2,1)} %param.35) | copy-start | bytes 3076
  1.0 4.3 %copy-start.6 = (bf16[512]{0:T(512)(128)(2,1)S(1)}, bf16[512]{0:T(512)(128)(2,1)}, u32[]{:S(2)}) copy-start(bf16[512]{0:T(512)(128)(2,1)} %param.34) | copy-start | bytes 3076
  1.0 4.3 %copy-start.7 = (bf16[512]{0:T(512)(128)(2,1)S(1)}, bf16[512]{0:T(512)(128)(2,1)}, u32[]{:S(2)}) copy-start(bf16[512]{0:T(512)(128)(2,1)} %param.28) | copy-start | bytes 3076
  1.0 4.3 %copy-start.8 = (bf16[512]{0:T(512)(128)(2,1)S(1)}, bf16[512]{0:T(512)(128)(2,1)}, u32[]{:S(2)}) copy-start(bf16[512]{0:T(512)(128)(2,1)} %param.27) | copy-start | bytes 3076
  1.0 4.9 %copy-start.2 = (bf16[3,1408]{1,0:T(4,128)(2,1)S(1)}, bf16[3,1408]{1,0:T(4,128)(2,1)}, u32[]{:S(2)}) copy-start(bf16[3,1408]{1,0:T(4,128)(2,1)} %param.32) | copy-start | bytes 25348
  1.0 4.9 %copy-start.3 = (bf16[3,1408]{1,0:T(4,128)(2,1)S(1)}, bf16[3,1408]{1,0:T(4,128)(2,1)}, u32[]{:S(2)}) copy-start(bf16[3,1408]{1,0:T(4,128)(2,1)} %param.31) | copy-start | bytes 25348

commit v2 on v1

--- a/solution.py
+++ b/solution.py
@@ -371,22 +371,25 @@
     load("proj", proj_in, proj)
     load("resid", resid_in, resid)
 
-    pl.semaphore_wait(barrier, n_sp * n_tp - 1)
-
-    half = R // 2
-    halo, halo_core = rc.ids(reach), rc.ids(reach)
+    with jax.named_scope("barrier"):
+        pl.semaphore_wait(barrier, n_sp * n_tp - 1)
+
+    part = R // n_tp
+    halo = rc.ids(reach)
+    halo_ids = rc.ids(3 * reach)
+
+    def quarter(k, tp):
+        return win.at[pl.ds(pl.multiple_of((reach - k) * R + tp * part, 16), part)]
 
     def halo_copy(k):
         return rc.make(
-            halo + k - 1,
-            pack_in.at[pl.ds(c * half, half)],
-            win.at[pl.ds((reach - k) * R + c * half, half)],
-            me_sp + k, me_tp,
+            halo + k - 1, pack_in.at[pl.ds(pl.multiple_of(me_tp * part, 16), part)],
+            quarter(k, me_tp), me_sp + k, me_tp,
         )
 
-    def halo_pass(k, core):
-        rows = win.at[pl.ds((reach - k) * R + core * half, half)]
-        return rc.make(halo_core + k - 1, rows, rows, me_sp, c_peer)
+    def halo_pass(k, kind, tp, tp_to):
+        rows = quarter(k, tp)
+        return rc.make(halo_ids + 3 * (k - 1) + kind, rows, rows, me_sp, tp_to)
 
     for k in range(1, reach + 1):
         start(halo_copy(k), me_sp + k < n_sp)
@@ -431,8 +434,8 @@
         slot = half_slot(w, p, z_sp[d] + 1 - 2 * x)
         return rc.make(x_ids[w] + d, slot, slot, x_peer, me_tp)
 
-    def send_z(w):
-        for d in list(range(2, nz)) + [1]:
+    def send_z(w, which):
+        for d in which:
             by_parity((odd + d) % 2, lambda p, d=d: z_weight(w, d, p).start())
 
     def send_x(w, d):
@@ -449,9 +452,20 @@
 
     for w in range(3):
         by_parity(odd, lambda p, w=w: own_weight(w, p).start())
-    send_x(0, 0)
-    send_z(0)
-    send_x(1, 0)
+    middle, near = list(range(2, nz)), [1]
+    rightward = 1 - z // (nz // 2)
+
+    inner = odd == rightward
+    outer = jnp.logical_not(inner)
+
+    def first_weights(right):
+        for w in range(2):
+            pl.when((1 - odd) == right)(lambda w=w: send_z(w, near))
+        pl.when(rightward == right)(lambda: send_z(0, middle))
+        for w in (1, 2):
+            pl.when((rightward == right) & inner)(lambda w=w: send_z(w, middle))
+
+    first_weights(0)
 
     @pl.when(odd == 1)
     def _():
@@ -471,25 +485,42 @@
         keys[rows, :] = jnp.dot(source, kup[...], preferred_element_type=f32).astype(bf16)
         vals[rows, :] = jnp.dot(source, vup[...], preferred_element_type=f32).astype(bf16)
 
-    raise_rows(reach)
+    with jax.named_scope("own_kv"):
+        raise_rows(reach)
     for k in range(1, reach + 1):
         @pl.when(me_sp >= k)
         def _(k=k):
-            halo_copy(k).wait_recv()
-            halo_pass(k, c).start()
+            with jax.named_scope("halo_wait"):
+                halo_copy(k).wait_recv()
+            halo_pass(k, 0, me_tp, y_peer).start()
+            halo_pass(k, 1, me_tp, c_peer).start()
 
         @pl.when(me_sp < k)
         def _(k=k):
             win[(reach - k) * R : (reach - k + 1) * R, :] = jnp.zeros((R, win.shape[1]), bf16)
-        sent.append((halo_pass(k, c), me_sp >= k))
+        sent.append((halo_pass(k, 0, me_tp, y_peer), me_sp >= k))
+        sent.append((halo_pass(k, 1, me_tp, c_peer), me_sp >= k))
     for k in range(1, reach + 1):
         @pl.when(me_sp >= k)
         def _(k=k):
-            halo_pass(k, 1 - c).wait_recv()
-
-    @pl.loop(0, reach)
-    def _(block):
-        raise_rows(block)
+            with jax.named_scope("halo_y_wait"):
+                halo_pass(k, 0, y_peer, y_peer).wait_recv()
+            halo_pass(k, 2, y_peer, c_peer).start()
+        sent.append((halo_pass(k, 2, y_peer, c_peer), me_sp >= k))
+    for k in range(1, reach + 1):
+        @pl.when(me_sp >= k)
+        def _(k=k):
+            with jax.named_scope("halo_core_wait"):
+                halo_pass(k, 1, c_peer, c_peer).wait_recv()
+                halo_pass(k, 2, far_peer, c_peer).wait_recv()
+    first_weights(1)
+    send_x(0, 0)
+    send_x(1, 0)
+
+    with jax.named_scope("kv"):
+        @pl.loop(0, reach)
+        def _(block):
+            raise_rows(block)
 
     side = win[:, latent_width:]
     side_f = side.astype(f32)
@@ -645,28 +676,54 @@
 
     loads["q"].wait()
     loads["t"].wait()
-    attend_chunk(0)
-    loads["proj"].wait()
-    loads["resid"].wait()
-    project(0)
-    for r in range(1, chunks):
-        attend_chunk(r)
-        mix_one(r - 1)
-        project(r)
-        norm_one(r - 1)
-    mix_one(chunks - 1)
-    norm_one(chunks - 1)
-    for d in range(1, nz):
-        send_x(0, d)
-    send_z(1)
-    send_z(2)
-    send_x(2, 0)
+    def z_left(w, d):
+        by_parity((odd + d) % 2, lambda p: z_weight(w, d, p).wait_send())
+
+    def forward(w, which):
+        for d in which:
+            with jax.named_scope("fwd%d_%d" % (w, d)):
+                send_x(w, d)
+
+    def attend_step(r):
+        with jax.named_scope("att"):
+            attend_chunk(r)
+        if r == 0:
+            loads["proj"].wait()
+            loads["resid"].wait()
+        else:
+            with jax.named_scope("mix"):
+                mix_one(r - 1)
+        with jax.named_scope("proj"):
+            project(r)
+        if r:
+            with jax.named_scope("norm"):
+                norm_one(r - 1)
+
     for r in range(chunks):
-        pass_pair(r)
-    for r in range(chunks):
-        pass_y(r)
-    for r in range(chunks):
-        rows_here(r)
+        attend_step(r)
+        if r == 0:
+            pl.when(outer)(lambda: send_z(1, middle))
+            forward(0, near)
+            send_x(2, 0)
+        elif r == 1:
+            forward(1, near)
+    forward(0, middle)
+    with jax.named_scope("mix"):
+        mix_one(chunks - 1)
+    with jax.named_scope("norm"):
+        norm_one(chunks - 1)
+    send_z(2, near)
+    forward(1, middle[:-1])
+    with jax.named_scope("pass_pair"):
+        for r in range(chunks):
+            pass_pair(r)
+    with jax.named_scope("pass_y"):
+        for r in range(chunks):
+            pass_y(r)
+    forward(1, middle[-1:])
+    with jax.named_scope("rows_here"):
+        for r in range(chunks):
+            rows_here(r)
 
     tile = 2 * LANES
     mid = first
@@ -683,12 +740,16 @@
                     .astype(f32)
                 )
 
-    all_here(0)
-    up(gate_w, 0)
-    for d in range(1, nz):
-        send_x(1, d)
-    all_here(1)
-    up(value_w, mid)
+    with jax.named_scope("wait_g"):
+        all_here(0)
+    with jax.named_scope("up_g"):
+        up(gate_w, 0)
+    forward(2, near)
+    with jax.named_scope("wait_v"):
+        all_here(1)
+    pl.when(outer)(lambda: send_z(2, middle))
+    with jax.named_scope("up_v"):
+        up(value_w, mid)
 
     tail_ids = rc.ids(2)
 
@@ -707,8 +768,7 @@
     def _():
         ext[0, 0:8, :] = jnp.zeros((8, ext.shape[2]), f32)
 
-    for d in range(1, nz):
-        send_x(2, d)
+    forward(2, middle)
 
     @pl.when((x == 1) | (z >= 2))
     def _():
@@ -718,35 +778,36 @@
 
     deep = 64
 
-    @pl.loop(0, 2)
-    def _(slot):
-        @pl.loop(0, R // deep)
-        def _(i):
-            at = pl.multiple_of(i * deep, 16)
-            marks = valid[slot, pl.ds(at, deep), :].astype(f32)
-            two, one = marks[:, LANES // 2 : LANES // 2 + 1], marks[:, LANES - 1 : LANES]
-
-            @pl.loop(0, first // tile)
-            def _(j):
-                cols = pl.multiple_of(j * tile, LANES)
-
-                def mixing(base, tap):
-                    rows = ext[slot, pl.ds(at, deep + 8), pl.ds(base + cols, tile)]
-                    weight = taps[pl.ds(tap, 8), pl.ds(cols, tile)]
-                    return (
-                        weight[0:1] * (pltpu.roll(rows, 2, 0)[8:] * two)
-                        + weight[1:2] * (pltpu.roll(rows, 1, 0)[8:] * one)
-                        + weight[2:3] * rows[8:]
-                    )
-
-                hid[slot, pl.ds(at, deep), pl.ds(cols, tile)] = (
-                    mixing(mid, 8) * jax.nn.gelu(mixing(0, 0))
-                ).astype(bf16)
-
-    all_here(2)
-
-    core_ids2, y_ids2, z_id2 = rc.ids(4), rc.ids(2), rc.ids()
+    with jax.named_scope("conv"):
+        @pl.loop(0, 2)
+        def _(slot):
+            @pl.loop(0, R // deep)
+            def _(i):
+                at = pl.multiple_of(i * deep, 16)
+                marks = valid[slot, pl.ds(at, deep), :].astype(f32)
+                two, one = marks[:, LANES // 2 : LANES // 2 + 1], marks[:, LANES - 1 : LANES]
+
+                @pl.loop(0, first // tile)
+                def _(j):
+                    cols = pl.multiple_of(j * tile, LANES)
+
+                    def mixing(base, tap):
+                        rows = ext[slot, pl.ds(at, deep + 8), pl.ds(base + cols, tile)]
+                        weight = taps[pl.ds(tap, 8), pl.ds(cols, tile)]
+                        return (
+                            weight[0:1] * (pltpu.roll(rows, 2, 0)[8:] * two)
+                            + weight[1:2] * (pltpu.roll(rows, 1, 0)[8:] * one)
+                            + weight[2:3] * rows[8:]
+                        )
+
+                    hid[slot, pl.ds(at, deep), pl.ds(cols, tile)] = (
+                        mixing(mid, 8) * jax.nn.gelu(mixing(0, 0))
+                    ).astype(bf16)
+
+    core_ids2, z_ids2, y_ids2 = rc.ids(4), rc.ids(2 * chunks), rc.ids(chunks)
     per = F // down_cols
+    half_z = (z // 2) % 2
+    slots = (1 - odd, odd)
 
     def down(slot, tp, target):
         for j in range(per):
@@ -754,45 +815,77 @@
                 hid[slot], down_w[per * tp + j], preferred_element_type=f32
             ).astype(bf16)
 
-    def to_core2(i, s):
+    def to_core2(f, s):
         return rc.make(
-            core_ids2 + 2 * i + s, core_out2.at[i, s], core_in2.at[i, s], me_sp, c_peer
+            core_ids2 + 2 * f + s, core_out2.at[f, s], core_in2.at[f, s], me_sp, c_peer
         )
 
-    def to_y2(s):
-        return rc.make(y_ids2 + s, y_out2.at[s], y_in2.at[s], me_sp, y_peer)
-
-    slots = (1 - odd, odd)
-    for i, yy in enumerate((1 - y, y)):
-        for s, slot in enumerate(slots):
-            down(slot, 2 * yy + 1 - c, core_out2.at[i, s])
-            start(to_core2(i, s))
-            down(slot, 2 * yy + c, keep2.at[i, s])
-            to_core2(i, s).wait_recv()
-            if i == 0:
-                y_out2[s] = (keep2[0, s].astype(f32) + core_in2[0, s].astype(f32)).astype(bf16)
-                start(to_y2(s))
-    to_y2(0).wait_recv()
-    z_out2[...] = (
-        keep2[1, 0].astype(f32) + core_in2[1, 0].astype(f32) + y_in2[0].astype(f32)
-    ).astype(bf16)
-    to_z2 = rc.make(z_id2, z_out2, z_in2, pair, me_tp)
-    start(to_z2)
-    to_y2(1).wait_recv()
-    to_z2.wait_recv()
+    def to_pair2(f, r):
+        at = pl.ds(r * C, C)
+        return rc.make(z_ids2 + chunks * f + r, z_out2.at[f, at], z_in2.at[f, at], pair, me_tp)
+
+    def to_y2(r):
+        at = pl.ds(r * C, C)
+        return rc.make(y_ids2 + r, y_out2.at[at], y_in2.at[at], me_sp, y_peer)
+
+    def down_set(f, ds):
+        yy = half_z if f == 0 else 1 - half_z
+        with jax.named_scope("wait_d%d" % f):
+            if f == 0:
+                by_parity(odd, lambda p: own_weight(2, p).wait())
+            for d in ds:
+                by_parity(odd, lambda p, d=d: x_landed(2, d, p).wait_recv())
+        with jax.named_scope("down"):
+            for s in range(2):
+                down(slots[s], 2 * yy + 1 - c, core_out2.at[f, s])
+                start(to_core2(f, s))
+            down(slots[0], 2 * yy + c, keep2.at[f, 0])
+        with jax.named_scope("core2_wait"):
+            to_core2(f, 0).wait_recv()
+        for r in range(chunks):
+            at = slice(r * C, (r + 1) * C)
+            z_out2[f, at, :] = (
+                keep2[f, 0, at, :].astype(f32) + core_in2[f, 0, at, :].astype(f32)
+            ).astype(bf16)
+            start(to_pair2(f, r))
+        with jax.named_scope("down"):
+            down(slots[1], 2 * yy + c, keep2.at[f, 1])
+        to_core2(f, 1).wait_recv()
+        for r in range(chunks):
+            at = slice(r * C, (r + 1) * C)
+            with jax.named_scope("z2_wait"):
+                to_pair2(f, r).wait_recv()
+
+            @pl.when(y != yy)
+            def _():
+                y_out2[at, :] = (
+                    keep2[f, 1, at, :].astype(f32)
+                    + core_in2[f, 1, at, :].astype(f32)
+                    + z_in2[f, at, :].astype(f32)
+                ).astype(bf16)
+                to_y2(r).start()
+
+    down_set(0, [0] + near)
+    down_set(1, middle)
+    mine = (y + half_z) % 2
     for r in range(chunks):
         at = slice(r * C, (r + 1) * C)
+        rows = pl.ds(r * C, C)
+        with jax.named_scope("y2_wait"):
+            to_y2(r).wait_recv()
+        sent.append((to_y2(r), None))
         mixed = residual_scale * rows_all[odd, at, features(me_tp)].astype(f32) + (
-            keep2[1, 1, at, :].astype(f32)
-            + core_in2[1, 1, at, :].astype(f32)
-            + y_in2[1, at, :].astype(f32)
-            + z_in2[at, :].astype(f32)
+            keep2[mine, 1, rows, :].astype(f32)
+            + core_in2[mine, 1, rows, :].astype(f32)
+            + z_in2[mine, rows, :].astype(f32)
+            + y_in2[at, :].astype(f32)
         )
         mix[at, :] = mixed
         send_stats(mixed, stat_ids2, stat_own2, stat_in2, r)
-    for r in range(chunks):
-        at = slice(r * C, (r + 1) * C)
-        out_ref[at, :] = norm(mix[at, :], stat_ids2, stat_own2, stat_in2, r, 2).astype(bf16)
+    with jax.named_scope("norm2"):
+        for r in range(chunks):
+            at = slice(r * C, (r + 1) * C)
+            out_ref[at, :] = norm(mix[at, :], stat_ids2, stat_own2, stat_in2, r, 2).astype(bf16)
 
     for copy, when in sent:
         if when is None:
@@ -802,7 +895,7 @@
     for w in range(3):
         for d in range(nz):
             if d:
-                by_parity((odd + d) % 2, lambda p, d=d, w=w: z_weight(w, d, p).wait_send())
+                z_left(w, d)
             by_parity(odd, lambda p, d=d, w=w: x_weight(w, d, p).wait_send())
     assert rc.count <= REMOTE, rc.count
 
@@ -875,7 +968,7 @@
             v(2, R, LANES),
             v(2, R, n_tp * F), v(n_sp * ffn_gate.shape[0], first), v(n_sp * ffn_gate.shape[0], first),
             v(n_sp, first, ffn_down.shape[1]), v(2, R + 8, 2 * first, dtype=f32), v(2, R, first),
-            v(2, 2, R, F), v(2, 2, R, F), v(2, 2, R, F), v(2, R, F), v(2, R, F), v(R, F), v(R, F),
+            v(2, 2, R, F), v(2, 2, R, F), v(2, 2, R, F), v(R, F), v(R, F), v(2, R, F), v(2, R, F),
             v(chunks, 8, LANES, dtype=f32), v(chunks, 3, 8, LANES, dtype=f32),
             pltpu.SemaphoreType.DMA((REMOTE,)), pltpu.SemaphoreType.DMA((REMOTE,)),
             pltpu.SemaphoreType.DMA((LOCAL,)),
@@ -894,8 +987,8 @@
     down_cols = arrays[15].shape[1]
     n_sp, n_tp = lax.axis_size("sp"), lax.axis_size("tp")
     paired = n_sp // 2
-    fits = n_tp == 4 and n_sp % 4 == 0 and paired & (paired - 1) == 0
-    tiled = rows % LANES == 0 and down_cols % LANES == 0 and features % down_cols == 0
+    fits = n_tp == 4 and paired == n_tp
+    tiled = rows % LANES == 0 and down_cols % LANES == 0 and features == 2 * down_cols
     return (fused if fits and tiled else plain)(*arrays)
 
 

time: 203 us -> 167 us (0.82)
  the two profiles are of different devices: /device:TPU:21 before, /device:TPU:29 now
where the time goes in v2:
time: 167 us
  Pallas kernels  159 us (95%)
  other arithmetic  2.96 us (2%)
  matrix products  2.81 us (2%)
  local copies, waits for them, and re-layouts  2.36 us (1%)
    pallas_call x1, Pallas kernels, fused(): pl.pallas_call(functools.partial(layer_kernel, sizes), in_specs=[hbm] * 7...  159 us

profile of v2, /device:TPU:29, one launch (start us, length us, event | category | flops | bytes accessed | tf_op | source)
XLA Modules:
  0.0 167.2 jit_solution(166395605495604801)
XLA Ops:
  0.0 0.0 copy-start.4
  0.0 0.0 copy-start.1
  0.0 0.0 copy-start
  0.0 0.8 multiply_cosine_fusion
  0.8 0.1 tile.20
  0.9 0.0 copy-start.5
  1.0 0.0 copy-start.6
  1.0 0.0 copy-start.7
  1.0 0.0 copy-start.8
  1.0 0.0 copy-start.2
  1.0 0.0 copy-start.3
  1.0 0.1 tile.8
  1.2 2.6 %fusion.2.t_in = bf16[384,512]{1,0:T(8,128)(2,1)} fusion(bf16[384,512]{1,0:T(8,128)(2,1)} %param.20, f32[48,8,4,128]{3,2,1,0:T(4,128)S(1)} %bitcast.26, f32[48,8,4,128]{3,2,1,0:T(4,128)S(1)} %bitcast.27, s32[512]{0:T(512)S(1)} %get-tuple-element.7, s32[512]{0:T(512)S(1)} %get-tuple-element.8, s32[512]{0:T(512)S(1)} %get-tuple-element.9, ...), kind=kOutput, calls=%fused_computation.5 | convolution fusion | flops 205193216 | bytes 2368000 | tf_op jit(solution)/shard_map/dot_general | solution.py:932
  3.8 0.0 copy-done.4
  3.8 0.1 broadcast_in_dim.41
  3.9 0.0 copy-done.1
  3.9 0.1 copy.20
  4.1 0.2 fusion.5
  4.3 0.0 copy-done
  4.3 0.9 pad_maximum_fusion.pack_in
  5.2 0.0 copy-done.5
  5.2 0.0 copy-done.6
  5.2 0.0 copy-done.7
  5.3 0.0 copy-done.8
  5.3 0.6 maximum_convert_fusion.gains
  5.9 0.0 copy-done.2
  5.9 0.0 copy-done.3
  6.0 0.6 fusion.18.taps
  6.6 158.8 %shard_map.172 = bf16[384,512]{1,0:T(8,128)(2,1)} custom-call(bf16[384,1024]{1,0:T(8,128)(2,1)} %q_in.1, bf16[384,512]{1,0:T(8,128)(2,1)} %fusion.2.t_in, bf16[384,640]{1,0:T(8,128)(2,1)} %pad_maximum_fusion.pack_in, bf16[512,1024]{1,0:T(8,128)(2,1)} %kup_in.1, bf16[512,1024]{1,0:T(8,128)(2,1)} %vup_in.1, bf16[1024,2048]{1,0:T(8,128)(2,1)} %proj_in.1, ...), custom_call_target="tpu_custom_call" | custom-call | tf_op jit(solution)/shard_map/pallas_call | solution.py:956
  165.5 1.8 %copy.29 = bf16[384,512]{1,0:T(8,128)(2,1)} copy(bf16[384,512]{1,0:T(8,128)(2,1)} %shard_map.172) | data formatting | bytes 786432
  (17 shorter events, 0.1 us)
Async XLA Ops:
  0.0 3.8 %copy-start.4 = (s32[384]{0:T(512)S(1)}, s32[384]{0:T(512)}, u32[]{:S(2)}) copy-start(s32[384]{0:T(512)} %param.23) | copy-start | bytes 4612
  0.0 3.9 %copy-start.1 = (bf16[384,64]{0,1:T(8,128)(2,1)S(1)}, bf16[384,64]{0,1:T(8,128)(2,1)}, u32[]{:S(2)}) copy-start(bf16[384,64]{0,1:T(8,128)(2,1)} %param.22) | copy-start | bytes 147460
  0.0 4.3 %copy-start = (bf16[384,512]{1,0:T(8,128)(2,1)S(1)}, bf16[384,512]{1,0:T(8,128)(2,1)}, u32[]{:S(2)}) copy-start(bf16[384,512]{1,0:T(8,128)(2,1)} %param.21) | copy-start | bytes 1179652
  0.9 4.3 %copy-start.5 = (bf16[512]{0:T(512)(128)(2,1)S(1)}, bf16[512]{0:T(512)(128)(2,1)}, u32[]{:S(2)}) copy-start(bf16[512]{0:T(512)(128)(2,1)} %param.35) | copy-start | bytes 3076
  1.0 4.3 %copy-start.6 = (bf16[512]{0:T(512)(128)(2,1)S(1)}, bf16[512]{0:T(512)(128)(2,1)}, u32[]{:S(2)}) copy-start(bf16[512]{0:T(512)(128)(2,1)} %param.34) | copy-start | bytes 3076
  1.0 4.3 %copy-start.7 = (bf16[512]{0:T(512)(128)(2,1)S(1)}, bf16[512]{0:T(512)(128)(2,1)}, u32[]{:S(2)}) copy-start(bf16[512]{0:T(512)(128)(2,1)} %param.28) | copy-start | bytes 3076
  1.0 4.3 %copy-start.8 = (bf16[512]{0:T(512)(128)(2,1)S(1)}, bf16[512]{0:T(512)(128)(2,1)}, u32[]{:S(2)}) copy-start(bf16[512]{0:T(512)(128)(2,1)} %param.27) | copy-start | bytes 3076
  1.0 4.9 %copy-start.2 = (bf16[3,1408]{1,0:T(4,128)(2,1)S(1)}, bf16[3,1408]{1,0:T(4,128)(2,1)}, u32[]{:S(2)}) copy-start(bf16[3,1408]{1,0:T(4,128)(2,1)} %param.32) | copy-start | bytes 25348
  1.0 4.9 %copy-start.3 = (bf16[3,1408]{1,0:T(4,128)(2,1)S(1)}, bf16[3,1408]{1,0:T(4,128)(2,1)}, u32[]{:S(2)}) copy-start(bf16[3,1408]{1,0:T(4,128)(2,1)} %param.31) | copy-start | bytes 25348

commit v3 on v2

--- a/solution.py
+++ b/solution.py
@@ -308,12 +308,13 @@
 
 def layer_kernel(
     sizes,
-    q_in, t_in, pack_in, kup_in, vup_in, proj_in, resid_in, gains, taps, gate_in, value_in, down_in,
+    q_in, t_in, latent_in, kup_in, vup_in, proj_in, resid_in, side_in, cosine, sine,
+    gain1, bias1, gain2, bias2, conv_g, conv_v, gate_in, value_in, down_in,
     out_ref,
-    win, q_v, t_v, kup, vup, proj, resid, keys, vals, ropes, bias, att,
+    taps, win, q_v, t_v, kup, vup, proj, resid, keys, vals, ropes, bias, att,
     core_out, core_in, keep, y_out, y_in, mix, stat_own, stat_in, valid,
     rows_all, gate_w, value_w, down_w, ext, hid,
-    core_out2, core_in2, keep2, y_out2, y_in2, z_out2, z_in2, stat_own2, stat_in2,
+    part2, core_in2, y_out2, y_in2, z_out2, z_in2, stat_own2, stat_in2,
     send_sems, recv_sems, local_sems,
 ):
     n_sp, n_tp, R, reach, heads, wide, first, second = sizes
@@ -363,7 +364,7 @@
         loads[name] = pltpu.make_async_copy(source, target, local_sems.at[len(loads)])
         loads[name].start()
 
-    load("win", pack_in, win.at[pl.ds(reach * R, R)])
+    load("win", latent_in, win.at[pl.ds(reach * R, R), pl.ds(0, latent_width)])
     load("kup", kup_in, kup)
     load("vup", vup_in, vup)
     load("q", q_in, q_v)
@@ -371,6 +372,22 @@
     load("proj", proj_in, proj)
     load("resid", resid_in, resid)
 
+    place = lax.broadcasted_iota(jnp.int32, (R, LANES), 1)
+    front = place % ROPE < ROPE // 2
+
+    def turn(vectors):
+        vectors = vectors.astype(f32)
+        swapped = jnp.where(
+            front,
+            pltpu.roll(vectors, LANES - ROPE // 2, 1),
+            pltpu.roll(vectors, ROPE // 2, 1),
+        )
+        return vectors * cosine[...] + swapped * sine[...]
+
+    own_rows = slice(reach * R, (reach + 1) * R)
+    win[own_rows, latent_width:] = jnp.where(
+        place < ROPE, turn(side_in[...]), side_in[...].astype(f32)
+    ).astype(bf16)
     with jax.named_scope("barrier"):
         pl.semaphore_wait(barrier, n_sp * n_tp - 1)
 
@@ -381,10 +398,20 @@
     def quarter(k, tp):
         return win.at[pl.ds(pl.multiple_of((reach - k) * R + tp * part, 16), part)]
 
+    halo_side = rc.ids(reach)
+    own_part = pl.multiple_of(me_tp * part, 16)
+
     def halo_copy(k):
         return rc.make(
-            halo + k - 1, pack_in.at[pl.ds(pl.multiple_of(me_tp * part, 16), part)],
-            quarter(k, me_tp), me_sp + k, me_tp,
+            halo + k - 1, latent_in.at[pl.ds(own_part, part)],
+            quarter(k, me_tp).at[:, pl.ds(0, latent_width)], me_sp + k, me_tp,
+        )
+
+    def halo_side_copy(k):
+        lanes = pl.ds(latent_width, LANES)
+        return rc.make(
+            halo_side + k - 1, win.at[pl.ds(reach * R + own_part, part), lanes],
+            quarter(k, me_tp).at[:, lanes], me_sp + k, me_tp,
         )
 
     def halo_pass(k, kind, tp, tp_to):
@@ -393,6 +420,7 @@
 
     for k in range(1, reach + 1):
         start(halo_copy(k), me_sp + k < n_sp)
+        start(halo_side_copy(k), me_sp + k < n_sp)
 
     halves = ((0, first), (first, second))
 
@@ -462,9 +490,11 @@
         for w in range(2):
             pl.when((1 - odd) == right)(lambda w=w: send_z(w, near))
         pl.when(rightward == right)(lambda: send_z(0, middle))
-        for w in (1, 2):
-            pl.when((rightward == right) & inner)(lambda w=w: send_z(w, middle))
-
+        pl.when((rightward == right) & inner)(lambda: send_z(1, middle))
+        pl.when((rightward == right) & inner)(lambda: send_z(2, middle[: len(middle) - right]))
+
+    send_x(0, 0)
+    send_x(1, 0)
     first_weights(0)
 
     @pl.when(odd == 1)
@@ -475,6 +505,14 @@
             value_w[:, second:] = jnp.zeros((gate_w.shape[0], blank), bf16)
             down_w[:, second:, :] = jnp.zeros((n_sp, blank, down_cols), bf16)
 
+    for conv, at in ((conv_g, 0), (conv_v, 8)):
+        def pick_taps(p, conv=conv, at=at):
+            first_unit, size = halves[p]
+            taps[at : at + CONV, 0:size] = conv[:, first_unit : first_unit + size].astype(f32)
+            if size < first:
+                taps[at : at + CONV, size:] = jnp.zeros((CONV, first - size), f32)
+        by_parity(odd, pick_taps)
+
     loads["win"].wait()
     loads["kup"].wait()
     loads["vup"].wait()
@@ -487,11 +525,17 @@
 
     with jax.named_scope("own_kv"):
         raise_rows(reach)
+    loads["q"].wait()
+    loads["t"].wait()
+    for duo in range(heads // 2):
+        cut = slice(duo * LANES, (duo + 1) * LANES)
+        t_v[:, cut] = turn(t_v[:, cut]).astype(bf16)
     for k in range(1, reach + 1):
         @pl.when(me_sp >= k)
         def _(k=k):
             with jax.named_scope("halo_wait"):
                 halo_copy(k).wait_recv()
+                halo_side_copy(k).wait_recv()
             halo_pass(k, 0, me_tp, y_peer).start()
             halo_pass(k, 1, me_tp, c_peer).start()
 
@@ -514,8 +558,6 @@
                 halo_pass(k, 1, c_peer, c_peer).wait_recv()
                 halo_pass(k, 2, far_peer, c_peer).wait_recv()
     first_weights(1)
-    send_x(0, 0)
-    send_x(1, 0)
 
     with jax.named_scope("kv"):
         @pl.loop(0, reach)
@@ -622,9 +664,9 @@
         total = jnp.concatenate([total] * (LANES // 8), 0).T
         row_mean = total[:, 0:1] / wide
         row_power = total[:, 4:5] / wide
-        return (values - row_mean) * lax.rsqrt(row_power - row_mean * row_mean + norm_eps) * gains[
-            gain : gain + 1, :
-        ] + gains[gain + 1 : gain + 2, :]
+        return (values - row_mean) * lax.rsqrt(row_power - row_mean * row_mean + norm_eps) * gain[0][
+            ...
+        ].astype(f32)[None, :] + gain[1][...].astype(f32)[None, :]
 
     def mix_one(r):
         at = slice(r * C, (r + 1) * C)
@@ -652,7 +694,7 @@
     def norm_one(r):
         at = slice(r * C, (r + 1) * C)
         rows_all[odd, at, features(me_tp)] = norm(
-            mix[at, :], stat_ids, stat_own, stat_in, r, 0
+            mix[at, :], stat_ids, stat_own, stat_in, r, (gain1, bias1)
         ).astype(bf16)
         start(to_pair(r, odd))
         start(y_gather(r, 1, odd, me_tp))
@@ -674,8 +716,6 @@
         core_gather(r, 5, odd, far_peer).wait_recv()
         core_gather(r, 6, 1 - odd, far_peer).wait_recv()
 
-    loads["q"].wait()
-    loads["t"].wait()
     def z_left(w, d):
         by_parity((odd + d) % 2, lambda p: z_weight(w, d, p).wait_send())
 
@@ -740,6 +780,7 @@
                     .astype(f32)
                 )
 
+    pl.when(outer & (rightward == 0))(lambda: send_z(2, middle))
     with jax.named_scope("wait_g"):
         all_here(0)
     with jax.named_scope("up_g"):
@@ -747,7 +788,7 @@
     forward(2, near)
     with jax.named_scope("wait_v"):
         all_here(1)
-    pl.when(outer)(lambda: send_z(2, middle))
+    pl.when(outer & (rightward == 1))(lambda: send_z(2, middle))
     with jax.named_scope("up_v"):
         up(value_w, mid)
 
@@ -763,25 +804,18 @@
     start(tail_copy(1, 1, x_peer), x == 0)
     start(tail_copy(0, 1, x_peer), x == 1)
     start(tail_copy(1, 0, me_sp + 3), (x == 1) & (z < nz - 2))
+    pl.when(inner & (rightward == 1))(lambda: send_z(2, middle[-1:]))
 
     @pl.when((x == 0) & (z < 2))
     def _():
         ext[0, 0:8, :] = jnp.zeros((8, ext.shape[2]), f32)
 
-    forward(2, middle)
-
-    @pl.when((x == 1) | (z >= 2))
-    def _():
-        tail_copy(0, 0, x_peer).wait_recv()
-    tail_copy(1, 1, x_peer).wait_recv()
-    rc.make(valid_id, valid.at[1 - odd], valid.at[1 - odd], pair, me_tp).wait_recv()
-
     deep = 64
 
-    with jax.named_scope("conv"):
+    def convolve(first_step, steps):
         @pl.loop(0, 2)
         def _(slot):
-            @pl.loop(0, R // deep)
+            @pl.loop(first_step, first_step + steps)
             def _(i):
                 at = pl.multiple_of(i * deep, 16)
                 marks = valid[slot, pl.ds(at, deep), :].astype(f32)
@@ -804,20 +838,27 @@
                         mixing(mid, 8) * jax.nn.gelu(mixing(0, 0))
                     ).astype(bf16)
 
+    rc.make(valid_id, valid.at[1 - odd], valid.at[1 - odd], pair, me_tp).wait_recv()
+    with jax.named_scope("conv"):
+        convolve(1, R // deep - 1)
+    forward(2, middle[:-1])
+    with jax.named_scope("tails"):
+        @pl.when((x == 1) | (z >= 2))
+        def _():
+            tail_copy(0, 0, x_peer).wait_recv()
+        tail_copy(1, 1, x_peer).wait_recv()
+    with jax.named_scope("conv_first"):
+        convolve(0, 1)
+
     core_ids2, z_ids2, y_ids2 = rc.ids(4), rc.ids(2 * chunks), rc.ids(chunks)
     per = F // down_cols
     half_z = (z // 2) % 2
     slots = (1 - odd, odd)
 
-    def down(slot, tp, target):
-        for j in range(per):
-            target[:, j * down_cols : (j + 1) * down_cols] = jnp.dot(
-                hid[slot], down_w[per * tp + j], preferred_element_type=f32
-            ).astype(bf16)
-
-    def to_core2(f, s):
+    def to_core2(d, s):
+        f = d // 2
         return rc.make(
-            core_ids2 + 2 * f + s, core_out2.at[f, s], core_in2.at[f, s], me_sp, c_peer
+            core_ids2 + 2 * f + s, part2.at[d, s], core_in2.at[f, s], me_sp, c_peer
         )
 
     def to_pair2(f, r):
@@ -828,45 +869,67 @@
         at = pl.ds(r * C, C)
         return rc.make(y_ids2 + r, y_out2.at[at], y_in2.at[at], me_sp, y_peer)
 
-    def down_set(f, ds):
-        yy = half_z if f == 0 else 1 - half_z
-        with jax.named_scope("wait_d%d" % f):
-            if f == 0:
+    def down_block(d):
+        f, block = d // 2, flip(z, d)
+        with jax.named_scope("wait_d%d" % d):
+            if d == 0:
                 by_parity(odd, lambda p: own_weight(2, p).wait())
-            for d in ds:
-                by_parity(odd, lambda p, d=d: x_landed(2, d, p).wait_recv())
+            by_parity(odd, lambda p: x_landed(2, d, p).wait_recv())
         with jax.named_scope("down"):
             for s in range(2):
-                down(slots[s], 2 * yy + 1 - c, core_out2.at[f, s])
-                start(to_core2(f, s))
-            down(slots[0], 2 * yy + c, keep2.at[f, 0])
-        with jax.named_scope("core2_wait"):
-            to_core2(f, 0).wait_recv()
-        for r in range(chunks):
-            at = slice(r * C, (r + 1) * C)
-            z_out2[f, at, :] = (
-                keep2[f, 0, at, :].astype(f32) + core_in2[f, 0, at, :].astype(f32)
-            ).astype(bf16)
-            start(to_pair2(f, r))
-        with jax.named_scope("down"):
-            down(slots[1], 2 * yy + c, keep2.at[f, 1])
-        to_core2(f, 1).wait_recv()
+                for j in range(per):
+                    part2[d, s, :, j * down_cols : (j + 1) * down_cols] = jnp.dot(
+                        hid[slots[s]], down_w[per * block + j], preferred_element_type=f32
+                    ).astype(bf16)
+                start(to_core2(d, s), block % 2 != c)
+
+    def pair_block(d):
+        f, block = d // 2, flip(z, d)
+
+        @pl.when(block % 2 == c)
+        def _():
+            with jax.named_scope("core2_wait"):
+                to_core2(d, 0).wait_recv()
+            for r in range(chunks):
+                at = slice(r * C, (r + 1) * C)
+                z_out2[f, at, :] = (
+                    part2[d, 0, at, :].astype(f32) + core_in2[f, 0, at, :].astype(f32)
+                ).astype(bf16)
+                to_pair2(f, r).start()
+            with jax.named_scope("core2_wait"):
+                to_core2(d, 1).wait_recv()
+
+    def mine_of(f):
+        return 2 * f + (odd + c) % 2
+
+    def pass_down(f):
+        yy = half_z if f == 0 else 1 - half_z
         for r in range(chunks):
             at = slice(r * C, (r + 1) * C)
             with jax.named_scope("z2_wait"):
                 to_pair2(f, r).wait_recv()
+            sent.append((to_pair2(f, r), None))
 
             @pl.when(y != yy)
             def _():
                 y_out2[at, :] = (
-                    keep2[f, 1, at, :].astype(f32)
+                    part2[mine_of(f), 1, pl.ds(r * C, C), :].astype(f32)
                     + core_in2[f, 1, at, :].astype(f32)
                     + z_in2[f, at, :].astype(f32)
                 ).astype(bf16)
                 to_y2(r).start()
 
-    down_set(0, [0] + near)
-    down_set(1, middle)
+    down_block(0)
+    down_block(1)
+    pair_block(0)
+    pair_block(1)
+    forward(2, middle[-1:])
+    down_block(2)
+    pass_down(0)
+    pair_block(2)
+    down_block(3)
+    pair_block(3)
+    pass_down(1)
     mine = (y + half_z) % 2
     for r in range(chunks):
         at = slice(r * C, (r + 1) * C)
@@ -875,7 +938,7 @@
             to_y2(r).wait_recv()
         sent.append((to_y2(r), None))
         mixed = residual_scale * rows_all[odd, at, features(me_tp)].astype(f32) + (
-            keep2[mine, 1, rows, :].astype(f32)
+            part2[mine_of(mine), 1, rows, :].astype(f32)
             + core_in2[mine, 1, rows, :].astype(f32)
             + z_in2[mine, rows, :].astype(f32)
             + y_in2[at, :].astype(f32)
@@ -885,7 +948,7 @@
     with jax.named_scope("norm2"):
         for r in range(chunks):
             at = slice(r * C, (r + 1) * C)
-            out_ref[at, :] = norm(mix[at, :], stat_ids2, stat_own2, stat_in2, r, 2).astype(bf16)
+            out_ref[at, :] = norm(mix[at, :], stat_ids2, stat_own2, stat_in2, r, (gain2, bias2)).astype(bf16)
 
     for copy, when in sent:
         if when is None:
@@ -919,31 +982,10 @@
     place = jnp.arange(LANES, dtype=jnp.int32) % half
     frequencies = 1.0 / rope_base_freq ** (2.0 * place.astype(f32) / ROPE)
     angles = positions.astype(f32)[:, None] * frequencies[None, :]
-    cosine, sine = jnp.cos(angles), jnp.sin(angles)
-
-    def turn(vectors):
-        width = vectors.shape[1]
-        row = lax.broadcasted_iota(jnp.int32, (width, width), 0)
-        col = lax.broadcasted_iota(jnp.int32, (width, width), 1)
-        front = col % ROPE < half
-        swap = jnp.where(front & (row == col + half), -1.0, 0.0) + jnp.where(
-            ~front & (row == col - half), 1.0, 0.0
-        )
-        swapped = jnp.dot(vectors, swap.astype(bf16), preferred_element_type=f32)
-        times = max(1, width // LANES)
-        cos_wide = jnp.tile(cosine, (1, times))[:, :width]
-        sin_wide = jnp.tile(sine, (1, times))[:, :width]
-        return (vectors.astype(f32) * cos_wide + swapped * sin_wide).astype(bf16)
-
-    packed = jnp.concatenate(
-        [latent, turn(rope_key), jnp.broadcast_to(doc_ids.astype(bf16)[:, None], (R, ROPE))], 1
-    )
-    gains = jnp.stack([norm1_gain, norm1_bias, norm2_gain, norm2_bias]).astype(f32)
-    odd = (lax.axis_index("sp") // 2) % 2
-    blank = jnp.zeros((5, units), f32)
-    taps = jnp.concatenate([conv_gate.astype(f32), blank, conv_value.astype(f32), blank], 0)
-    taps = jnp.where(
-        odd == 0, taps[:, :first], jnp.pad(taps[:, first:], ((0, 0), (0, first - second)))
+    front = jnp.arange(LANES) % ROPE < half
+    cosine, sine = jnp.cos(angles), jnp.where(front, -1.0, 1.0) * jnp.sin(angles)
+    side = jnp.concatenate(
+        [rope_key, jnp.broadcast_to(doc_ids.astype(bf16)[:, None], (R, LANES - ROPE))], 1
     )
     hbm = pl.BlockSpec(memory_space=pl.ANY)
     vmem = pl.BlockSpec(memory_space=pltpu.VMEM)
@@ -955,11 +997,11 @@
     C = LANES
     return pl.pallas_call(
         functools.partial(layer_kernel, sizes),
-        in_specs=[hbm] * 7 + [vmem] * 2 + [hbm] * 3,
+        in_specs=[hbm] * 7 + [vmem] * 9 + [hbm] * 3,
         out_specs=vmem,
         out_shape=jax.ShapeDtypeStruct((R, F), bf16),
         scratch_shapes=[
-            v(window, packed.shape[1]), v(R, heads * NOPE), v(R, heads * ROPE),
+            v(16, first, dtype=f32), v(window, latent.shape[1] + LANES), v(R, heads * NOPE), v(R, heads * ROPE),
             v(*key_up.shape), v(*value_up.shape), v(*out_proj.shape), v(R, F),
             v(window, heads * NOPE), v(window, heads * VDIM), v(2, window, LANES),
             v(R, window, dtype=f32), v(R, heads * VDIM),
@@ -968,7 +1010,7 @@
             v(2, R, LANES),
             v(2, R, n_tp * F), v(n_sp * ffn_gate.shape[0], first), v(n_sp * ffn_gate.shape[0], first),
             v(n_sp, first, ffn_down.shape[1]), v(2, R + 8, 2 * first, dtype=f32), v(2, R, first),
-            v(2, 2, R, F), v(2, 2, R, F), v(2, 2, R, F), v(R, F), v(R, F), v(2, R, F), v(2, R, F),
+            v(4, 2, R, F), v(2, 2, R, F), v(R, F), v(R, F), v(2, R, F), v(2, R, F),
             v(chunks, 8, LANES, dtype=f32), v(chunks, 3, 8, LANES, dtype=f32),
             pltpu.SemaphoreType.DMA((REMOTE,)), pltpu.SemaphoreType.DMA((REMOTE,)),
             pltpu.SemaphoreType.DMA((LOCAL,)),
@@ -977,8 +1019,9 @@
             collective_id=0, has_side_effects=True, vmem_limit_bytes=64 * 1024 * 1024 - 65536
         ),
     )(
-        query_nope, turn(query_rope), packed, key_up, value_up, out_proj, residual, gains, taps,
-        ffn_gate, ffn_value, ffn_down,
+        query_nope, query_rope, latent, key_up, value_up, out_proj, residual, side, cosine, sine,
+        norm1_gain, norm1_bias, norm2_gain, norm2_bias,
+        conv_gate, conv_value, ffn_gate, ffn_value, ffn_down,
     )
 
 

time: 167 us -> 154 us (0.922)
  the two profiles are of different devices: /device:TPU:29 before, /device:TPU:21 now
where the time goes in v3:
time: 154 us
  Pallas kernels  148 us (96%)
  other arithmetic  2.94 us (2%)
  local copies, waits for them, and re-layouts  2.8 us (2%)
    pallas_call x1, Pallas kernels, fused(): pl.pallas_call(functools.partial(layer_kernel, sizes), in_specs=[hbm] * 7...  148 us

profile of v3, /device:TPU:21, one launch (start us, length us, event | category | flops | bytes accessed | tf_op | source)
XLA Modules:
  0.0 153.7 jit_solution(4228453260934421910)
XLA Ops:
  0.0 0.7 convert_element_type.17
  0.7 0.1 broadcast_in_dim.8
  0.8 0.9 copy.19
  1.7 0.7 pad_maximum_fusion.side_in
  2.5 1.5 fusion
  4.0 147.9 %shard_map.172 = bf16[384,512]{1,0:T(8,128)(2,1)} custom-call(bf16[384,1024]{1,0:T(8,128)(2,1)} %q_in.1, bf16[384,512]{1,0:T(8,128)(2,1)} %t_in.1, bf16[384,512]{1,0:T(8,128)(2,1)} %latent_in.1, bf16[512,1024]{1,0:T(8,128)(2,1)} %kup_in.1, bf16[512,1024]{1,0:T(8,128)(2,1)} %vup_in.1, bf16[1024,2048]{1,0:T(8,128)(2,1)} %proj_in.1, bf16[384,512]{1,0:T(8,128)(2,1)} %resid_in.1, ...), custom_call_target="tpu_custom_call" | custom-call | tf_op jit(solution)/shard_map/pallas_call | solution.py:998
  151.9 1.8 %copy.21 = bf16[384,512]{1,0:T(8,128)(2,1)} copy(bf16[384,512]{1,0:T(8,128)(2,1)} %shard_map.172) | data formatting | bytes 786432
  (2 shorter events, 0.0 us)

commit v4 on v3

--- a/solution.py
+++ b/solution.py
@@ -308,10 +308,10 @@
 
 def layer_kernel(
     sizes,
-    q_in, t_in, latent_in, kup_in, vup_in, proj_in, resid_in, side_in, cosine, sine,
+    q_in, t_in, latent_in, kup_in, vup_in, proj_in, resid_in, rope_in, doc_in, cosine, sine,
     gain1, bias1, gain2, bias2, conv_g, conv_v, gate_in, value_in, down_in,
     out_ref,
-    taps, win, q_v, t_v, kup, vup, proj, resid, keys, vals, ropes, bias, att,
+    side_v, taps, win, q_v, t_v, kup, vup, proj, resid, keys, vals, ropes, bias, att,
     core_out, core_in, keep, y_out, y_in, mix, stat_own, stat_in, valid,
     rows_all, gate_w, value_w, down_w, ext, hid,
     part2, core_in2, y_out2, y_in2, z_out2, z_in2, stat_own2, stat_in2,
@@ -385,8 +385,12 @@
         return vectors * cosine[...] + swapped * sine[...]
 
     own_rows = slice(reach * R, (reach + 1) * R)
+    for r in range(chunks):
+        docs = doc_in[pl.ds(r * C, C)].astype(f32)
+        side_v[r * C : (r + 1) * C, 0:ROPE] = rope_in[:, r * C : (r + 1) * C].astype(f32).T
+        side_v[r * C : (r + 1) * C, ROPE:] = jnp.broadcast_to(docs[None, :], (C, C)).T[:, ROPE:]
     win[own_rows, latent_width:] = jnp.where(
-        place < ROPE, turn(side_in[...]), side_in[...].astype(f32)
+        place < ROPE, turn(side_v[...]), side_v[...]
     ).astype(bf16)
     with jax.named_scope("barrier"):
         pl.semaphore_wait(barrier, n_sp * n_tp - 1)
@@ -426,14 +430,14 @@
 
     def half_in(w, parity):
         at, size = halves[parity]
-        if w == 2:
-            return down_in.at[pl.ds(at, size), :]
+        if w >= 2:
+            return down_in.at[pl.ds(at + (w - 2) * (size // 2), size // 2), :]
         return (gate_in, value_in)[w].at[:, pl.ds(at, size)]
 
     def half_slot(w, parity, owner):
         size = halves[parity][1]
-        if w == 2:
-            return down_w.at[owner, pl.ds(0, size), :]
+        if w >= 2:
+            return down_w.at[owner, pl.ds((w - 2) * (size // 2), size // 2), :]
         rows = pl.ds(pl.multiple_of(owner * gate_rows, 16), gate_rows)
         return (gate_w, value_w)[w].at[rows, pl.ds(0, size)]
 
@@ -441,9 +445,10 @@
         for p in range(2):
             pl.when(parity == p)(functools.partial(act, p))
 
-    z_ids = [rc.ids(nz) for _ in range(3)]
-    x_ids = [rc.ids(nz) for _ in range(3)]
-    own_ids = [len(loads) + w for w in range(3)]
+    pieces = ((0,), (1,), (2, 3))
+    z_ids = [rc.ids(nz) for _ in range(4)]
+    x_ids = [rc.ids(nz) for _ in range(4)]
+    own_ids = [len(loads) + w for w in range(4)]
 
     def own_weight(w, p):
         return pltpu.make_async_copy(half_in(w, p), half_slot(w, p, me_sp), local_sems.at[own_ids[w]])
@@ -464,12 +469,18 @@
 
     def send_z(w, which):
         for d in which:
-            by_parity((odd + d) % 2, lambda p, d=d: z_weight(w, d, p).start())
+            def act(p, d=d):
+                for piece in pieces[w]:
+                    z_weight(piece, d, p).start()
+            by_parity((odd + d) % 2, act)
 
     def send_x(w, d):
-        if d:
-            by_parity(odd, lambda p: z_landed(w, d, p).wait_recv())
-        by_parity(odd, lambda p: x_weight(w, d, p).start())
+        def act(p):
+            for piece in pieces[w]:
+                if d:
+                    z_landed(piece, d, p).wait_recv()
+                x_weight(piece, d, p).start()
+        by_parity(odd, act)
 
     def all_here(w):
         def act(p):
@@ -478,7 +489,7 @@
                 x_landed(w, d, p).wait_recv()
         by_parity(odd, act)
 
-    for w in range(3):
+    for w in range(4):
         by_parity(odd, lambda p, w=w: own_weight(w, p).start())
     middle, near = list(range(2, nz)), [1]
     rightward = 1 - z // (nz // 2)
@@ -489,9 +500,14 @@
     def first_weights(right):
         for w in range(2):
             pl.when((1 - odd) == right)(lambda w=w: send_z(w, near))
-        pl.when(rightward == right)(lambda: send_z(0, middle))
-        pl.when((rightward == right) & inner)(lambda: send_z(1, middle))
-        pl.when((rightward == right) & inner)(lambda: send_z(2, middle[: len(middle) - right]))
+        pl.when((rightward == right) & outer)(lambda: send_z(0, middle))
+        if not right:
+            def inner_weights(turned):
+                send_z(0, middle)
+                send_z(1, middle)
+                send_z(2, middle[: len(middle) - turned])
+            for turned in range(2):
+                pl.when(inner & (rightward == turned))(functools.partial(inner_weights, turned))
 
     send_x(0, 0)
     send_x(1, 0)
@@ -664,9 +680,8 @@
         total = jnp.concatenate([total] * (LANES // 8), 0).T
         row_mean = total[:, 0:1] / wide
         row_power = total[:, 4:5] / wide
-        return (values - row_mean) * lax.rsqrt(row_power - row_mean * row_mean + norm_eps) * gain[0][
-            ...
-        ].astype(f32)[None, :] + gain[1][...].astype(f32)[None, :]
+        scaled = (values - row_mean) * lax.rsqrt(row_power - row_mean * row_mean + norm_eps)
+        return scaled * gain[0][...].astype(f32)[None, :] + gain[1][...].astype(f32)[None, :]
 
     def mix_one(r):
         at = slice(r * C, (r + 1) * C)
@@ -788,7 +803,7 @@
     forward(2, near)
     with jax.named_scope("wait_v"):
         all_here(1)
-    pl.when(outer & (rightward == 1))(lambda: send_z(2, middle))
+    pl.when(outer & (rightward == 1))(lambda: send_z(2, middle[:-1]))
     with jax.named_scope("up_v"):
         up(value_w, mid)
 
@@ -804,7 +819,7 @@
     start(tail_copy(1, 1, x_peer), x == 0)
     start(tail_copy(0, 1, x_peer), x == 1)
     start(tail_copy(1, 0, me_sp + 3), (x == 1) & (z < nz - 2))
-    pl.when(inner & (rightward == 1))(lambda: send_z(2, middle[-1:]))
+    pl.when(rightward == 1)(lambda: send_z(2, middle[-1:]))
 
     @pl.when((x == 0) & (z < 2))
     def _():
@@ -872,9 +887,12 @@
     def down_block(d):
         f, block = d // 2, flip(z, d)
         with jax.named_scope("wait_d%d" % d):
-            if d == 0:
-                by_parity(odd, lambda p: own_weight(2, p).wait())
-            by_parity(odd, lambda p: x_landed(2, d, p).wait_recv())
+            def act(p):
+                for piece in pieces[2]:
+                    if d == 0:
+                        own_weight(piece, p).wait()
+                    x_landed(piece, d, p).wait_recv()
+            by_parity(odd, act)
         with jax.named_scope("down"):
             for s in range(2):
                 for j in range(per):
@@ -925,10 +943,10 @@
     pair_block(1)
     forward(2, middle[-1:])
     down_block(2)
-    pass_down(0)
     pair_block(2)
     down_block(3)
     pair_block(3)
+    pass_down(0)
     pass_down(1)
     mine = (y + half_z) % 2
     for r in range(chunks):
@@ -955,7 +973,7 @@
             copy.wait_send()
         else:
             pl.when(when)(copy.wait_send)
-    for w in range(3):
+    for w in range(4):
         for d in range(nz):
             if d:
                 z_left(w, d)
@@ -984,9 +1002,6 @@
     angles = positions.astype(f32)[:, None] * frequencies[None, :]
     front = jnp.arange(LANES) % ROPE < half
     cosine, sine = jnp.cos(angles), jnp.where(front, -1.0, 1.0) * jnp.sin(angles)
-    side = jnp.concatenate(
-        [rope_key, jnp.broadcast_to(doc_ids.astype(bf16)[:, None], (R, LANES - ROPE))], 1
-    )
     hbm = pl.BlockSpec(memory_space=pl.ANY)
     vmem = pl.BlockSpec(memory_space=pltpu.VMEM)
     sizes = (n_sp, n_tp, R, REACH, heads, n_tp * F, first, second)
@@ -997,11 +1012,11 @@
     C = LANES
     return pl.pallas_call(
         functools.partial(layer_kernel, sizes),
-        in_specs=[hbm] * 7 + [vmem] * 9 + [hbm] * 3,
+        in_specs=[hbm] * 7 + [vmem] * 10 + [hbm] * 3,
         out_specs=vmem,
         out_shape=jax.ShapeDtypeStruct((R, F), bf16),
         scratch_shapes=[
-            v(16, first, dtype=f32), v(window, latent.shape[1] + LANES), v(R, heads * NOPE), v(R, heads * ROPE),
+            v(R, LANES, dtype=f32), v(16, first, dtype=f32), v(window, latent.shape[1] + LANES), v(R, heads * NOPE), v(R, heads * ROPE),
             v(*key_up.shape), v(*value_up.shape), v(*out_proj.shape), v(R, F),
             v(window, heads * NOPE), v(window, heads * VDIM), v(2, window, LANES),
             v(R, window, dtype=f32), v(R, heads * VDIM),
@@ -1019,7 +1034,7 @@
             collective_id=0, has_side_effects=True, vmem_limit_bytes=64 * 1024 * 1024 - 65536
         ),
     )(
-        query_nope, query_rope, latent, key_up, value_up, out_proj, residual, side, cosine, sine,
+        query_nope, query_rope, latent, key_up, value_up, out_proj, residual, rope_key.T, doc_ids, cosine, sine,
         norm1_gain, norm1_bias, norm2_gain, norm2_bias,
         conv_gate, conv_value, ffn_gate, ffn_value, ffn_down,
     )

time: 154 us -> 141 us (0.916)
  Pallas kernels: 148 us -> 137 us
    pallas_call x1, Pallas kernels: 148 us -> 137 us  [fused(): pl.pallas_call(functools.partial(layer_kernel, sizes), in_specs=[hbm] * 7...]
where the time goes in v4:
time: 141 us; the launch traced here: 140 us
  Pallas kernels  137 us (97%)
  local copies, waits for them, and re-layouts  1.77 us (1%)
  other arithmetic  1.52 us (1%)
    pallas_call x1, Pallas kernels, fused(): pl.pallas_call(functools.partial(layer_kernel, sizes), in_specs=[hbm] * 7...  137 us

profile of v4, /device:TPU:21, one launch (start us, length us, event | category | flops | bytes accessed | tf_op | source)
XLA Modules:
  0.0 140.0 jit_solution(13970344079457353973)
XLA Ops:
  0.0 1.5 %fusion = (f32[384,128]{1,0:T(8,128)}, f32[384,128]{1,0:T(8,128)}) fusion(f32[128]{0:T(128)S(1)} %get-tuple-element.7, f32[128]{0:T(128)S(1)} %get-tuple-element.8, f32[384]{0:T(512)S(1)} %add_convert_fusion), kind=kLoop, calls=%fused_computation.2 | loop fusion | flops 98304 | bytes 395776 | tf_op jit(solution)/shard_map/mul | solution.py:1004
  1.5 136.7 %shard_map.172 = bf16[384,512]{1,0:T(8,128)(2,1)} custom-call(bf16[384,1024]{1,0:T(8,128)(2,1)} %q_in.1, bf16[384,512]{1,0:T(8,128)(2,1)} %t_in.1, bf16[384,512]{1,0:T(8,128)(2,1)} %latent_in.1, bf16[512,1024]{1,0:T(8,128)(2,1)} %kup_in.1, bf16[512,1024]{1,0:T(8,128)(2,1)} %vup_in.1, bf16[1024,2048]{1,0:T(8,128)(2,1)} %proj_in.1, bf16[384,512]{1,0:T(8,128)(2,1)} %resid_in.1, ...), custom_call_target="tpu_custom_call" | custom-call | tf_op jit(solution)/shard_map/pallas_call | solution.py:1013
  138.2 1.8 %copy.20 = bf16[384,512]{1,0:T(8,128)(2,1)} copy(bf16[384,512]{1,0:T(8,128)(2,1)} %shard_map.172) | data formatting | bytes 786432
  (2 shorter events, 0.0 us)

commit v5 on v4

--- a/solution.py
+++ b/solution.py
@@ -2,6 +2,7 @@
 
 import jax
 import jax.numpy as jnp
+import numpy as np
 from jax import lax
 from jax.experimental import pallas as pl
 from jax.experimental.pallas import tpu as pltpu
@@ -308,10 +309,10 @@
 
 def layer_kernel(
     sizes,
-    q_in, t_in, latent_in, kup_in, vup_in, proj_in, resid_in, rope_in, doc_in, cosine, sine,
+    q_in, t_in, latent_in, kup_in, vup_in, proj_in, resid_in, rope_in, doc_in, frequencies,
     gain1, bias1, gain2, bias2, conv_g, conv_v, gate_in, value_in, down_in,
     out_ref,
-    side_v, taps, win, q_v, t_v, kup, vup, proj, resid, keys, vals, ropes, bias, att,
+    cosine, sine, side_v, taps, win, q_v, t_v, kup, vup, proj, resid, keys, vals, ropes, bias, att,
     core_out, core_in, keep, y_out, y_in, mix, stat_own, stat_in, valid,
     rows_all, gate_w, value_w, down_w, ext, hid,
     part2, core_in2, y_out2, y_in2, z_out2, z_in2, stat_own2, stat_in2,
@@ -372,8 +373,45 @@
     load("proj", proj_in, proj)
     load("resid", resid_in, resid)
 
+    with jax.named_scope("barrier"):
+        pl.semaphore_wait(barrier, n_sp * n_tp - 1)
+
+    part = R // n_tp
+    halo = rc.ids(reach)
+    halo_ids = rc.ids(3 * reach)
+
+    def quarter(k, tp):
+        return win.at[pl.ds(pl.multiple_of((reach - k) * R + tp * part, 16), part)]
+
+    halo_side = rc.ids(reach)
+    own_part = pl.multiple_of(me_tp * part, 16)
+
+    def halo_copy(k):
+        return rc.make(
+            halo + k - 1, latent_in.at[pl.ds(own_part, part)],
+            quarter(k, me_tp).at[:, pl.ds(0, latent_width)], me_sp + k, me_tp,
+        )
+
+    def halo_side_copy(k):
+        lanes = pl.ds(latent_width, LANES)
+        return rc.make(
+            halo_side + k - 1, win.at[pl.ds(reach * R + own_part, part), lanes],
+            quarter(k, me_tp).at[:, lanes], me_sp + k, me_tp,
+        )
+
+    def halo_pass(k, kind, tp, tp_to):
+        rows = quarter(k, tp)
+        return rc.make(halo_ids + 3 * (k - 1) + kind, rows, rows, me_sp, tp_to)
+
+    for k in range(1, reach + 1):
+        start(halo_copy(k), me_sp + k < n_sp)
+
     place = lax.broadcasted_iota(jnp.int32, (R, LANES), 1)
     front = place % ROPE < ROPE // 2
+    row_at = lax.broadcasted_iota(jnp.int32, (R, LANES), 0) + me_sp * R
+    angles = row_at.astype(f32) * frequencies[...]
+    cosine[...] = jnp.cos(angles)
+    sine[...] = jnp.where(front, -1.0, 1.0) * jnp.sin(angles)
 
     def turn(vectors):
         vectors = vectors.astype(f32)
@@ -392,39 +430,9 @@
     win[own_rows, latent_width:] = jnp.where(
         place < ROPE, turn(side_v[...]), side_v[...]
     ).astype(bf16)
-    with jax.named_scope("barrier"):
-        pl.semaphore_wait(barrier, n_sp * n_tp - 1)
-
-    part = R // n_tp
-    halo = rc.ids(reach)
-    halo_ids = rc.ids(3 * reach)
-
-    def quarter(k, tp):
-        return win.at[pl.ds(pl.multiple_of((reach - k) * R + tp * part, 16), part)]
-
-    halo_side = rc.ids(reach)
-    own_part = pl.multiple_of(me_tp * part, 16)
-
-    def halo_copy(k):
-        return rc.make(
-            halo + k - 1, latent_in.at[pl.ds(own_part, part)],
-            quarter(k, me_tp).at[:, pl.ds(0, latent_width)], me_sp + k, me_tp,
-        )
-
-    def halo_side_copy(k):
-        lanes = pl.ds(latent_width, LANES)
-        return rc.make(
-            halo_side + k - 1, win.at[pl.ds(reach * R + own_part, part), lanes],
-            quarter(k, me_tp).at[:, lanes], me_sp + k, me_tp,
-        )
-
-    def halo_pass(k, kind, tp, tp_to):
-        rows = quarter(k, tp)
-        return rc.make(halo_ids + 3 * (k - 1) + kind, rows, rows, me_sp, tp_to)
-
     for k in range(1, reach + 1):
-        start(halo_copy(k), me_sp + k < n_sp)
         start(halo_side_copy(k), me_sp + k < n_sp)
+
 
     halves = ((0, first), (first, second))
 
@@ -574,6 +582,7 @@
                 halo_pass(k, 1, c_peer, c_peer).wait_recv()
                 halo_pass(k, 2, far_peer, c_peer).wait_recv()
     first_weights(1)
+    send_x(2, 0)
 
     with jax.named_scope("kv"):
         @pl.loop(0, reach)
@@ -759,7 +768,6 @@
         if r == 0:
             pl.when(outer)(lambda: send_z(1, middle))
             forward(0, near)
-            send_x(2, 0)
         elif r == 1:
             forward(1, near)
     forward(0, middle)
@@ -800,10 +808,10 @@
         all_here(0)
     with jax.named_scope("up_g"):
         up(gate_w, 0)
+    pl.when(outer & (rightward == 1))(lambda: send_z(2, middle[:-1]))
     forward(2, near)
     with jax.named_scope("wait_v"):
         all_here(1)
-    pl.when(outer & (rightward == 1))(lambda: send_z(2, middle[:-1]))
     with jax.named_scope("up_v"):
         up(value_w, mid)
 
@@ -994,14 +1002,9 @@
     window = (REACH + 1) * R
     chunks = R // LANES
     f32, bf16 = jnp.float32, jnp.bfloat16
-    offset = lax.axis_index("sp") * R
-    positions = offset + jnp.arange(R, dtype=jnp.int32)
     half = ROPE // 2
-    place = jnp.arange(LANES, dtype=jnp.int32) % half
-    frequencies = 1.0 / rope_base_freq ** (2.0 * place.astype(f32) / ROPE)
-    angles = positions.astype(f32)[:, None] * frequencies[None, :]
-    front = jnp.arange(LANES) % ROPE < half
-    cosine, sine = jnp.cos(angles), jnp.where(front, -1.0, 1.0) * jnp.sin(angles)
+    place = np.arange(LANES) % half
+    frequencies = jnp.asarray((rope_base_freq ** (-2.0 * place / ROPE))[None, :], f32)
     hbm = pl.BlockSpec(memory_space=pl.ANY)
     vmem = pl.BlockSpec(memory_space=pltpu.VMEM)
     sizes = (n_sp, n_tp, R, REACH, heads, n_tp * F, first, second)
@@ -1012,11 +1015,11 @@
     C = LANES
     return pl.pallas_call(
         functools.partial(layer_kernel, sizes),
-        in_specs=[hbm] * 7 + [vmem] * 10 + [hbm] * 3,
+        in_specs=[hbm] * 7 + [vmem] * 9 + [hbm] * 3,
         out_specs=vmem,
         out_shape=jax.ShapeDtypeStruct((R, F), bf16),
         scratch_shapes=[
-            v(R, LANES, dtype=f32), v(16, first, dtype=f32), v(window, latent.shape[1] + LANES), v(R, heads * NOPE), v(R, heads * ROPE),
+            v(R, LANES, dtype=f32), v(R, LANES, dtype=f32), v(R, LANES, dtype=f32), v(16, first, dtype=f32), v(window, latent.shape[1] + LANES), v(R, heads * NOPE), v(R, heads * ROPE),
             v(*key_up.shape), v(*value_up.shape), v(*out_proj.shape), v(R, F),
             v(window, heads * NOPE), v(window, heads * VDIM), v(2, window, LANES),
             v(R, window, dtype=f32), v(R, heads * VDIM),
@@ -1034,7 +1037,7 @@
             collective_id=0, has_side_effects=True, vmem_limit_bytes=64 * 1024 * 1024 - 65536
         ),
     )(
-        query_nope, query_rope, latent, key_up, value_up, out_proj, residual, rope_key.T, doc_ids, cosine, sine,
+        query_nope, query_rope, latent, key_up, value_up, out_proj, residual, rope_key.T, doc_ids, frequencies,
         norm1_gain, norm1_bias, norm2_gain, norm2_bias,
         conv_gate, conv_value, ffn_gate, ffn_value, ffn_down,
     )

time: 141 us -> 140 us (level)
  other arithmetic: 1.52 us -> 0 us
    mul x1 -> x0, other arithmetic: 1.51 us -> none  [fused(): jnp.where(front, -1.0, 1.0) * jnp.sin(angles)]
where the time goes in v5:
time: 140 us
  Pallas kernels  138 us (99%)
  local copies, waits for them, and re-layouts  1.77 us (1%)
    pallas_call x1, Pallas kernels, fused(): pl.pallas_call(functools.partial(layer_kernel, sizes), in_specs=[hbm] * 7...  138 us

profile of v5, /device:TPU:21, one launch (start us, length us, event | category | flops | bytes accessed | tf_op | source)
XLA Modules:
  0.0 139.5 jit_solution(12997758637670027891)
XLA Ops:
  0.0 137.8 %shard_map.181 = bf16[384,512]{1,0:T(8,128)(2,1)} custom-call(bf16[384,1024]{1,0:T(8,128)(2,1)} %q_in.1, bf16[384,512]{1,0:T(8,128)(2,1)} %t_in.1, bf16[384,512]{1,0:T(8,128)(2,1)} %latent_in.1, bf16[512,1024]{1,0:T(8,128)(2,1)} %kup_in.1, bf16[512,1024]{1,0:T(8,128)(2,1)} %vup_in.1, bf16[1024,2048]{1,0:T(8,128)(2,1)} %proj_in.1, bf16[384,512]{1,0:T(8,128)(2,1)} %resid_in.1, ...), custom_call_target="tpu_custom_call" | custom-call | tf_op jit(solution)/shard_map/pallas_call | solution.py:1016
  137.8 1.8 %copy.21 = bf16[384,512]{1,0:T(8,128)(2,1)} copy(bf16[384,512]{1,0:T(8,128)(2,1)} %shard_map.181) | data formatting | bytes 786432

commit v6 on v5

--- a/solution.py
+++ b/solution.py
@@ -515,7 +515,8 @@
                 send_z(1, middle)
                 send_z(2, middle[: len(middle) - turned])
             for turned in range(2):
-                pl.when(inner & (rightward == turned))(functools.partial(inner_weights, turned))
+                held = rightward * x
+                pl.when(inner & (held == turned))(functools.partial(inner_weights, turned))
 
     send_x(0, 0)
     send_x(1, 0)
@@ -827,7 +828,7 @@
     start(tail_copy(1, 1, x_peer), x == 0)
     start(tail_copy(0, 1, x_peer), x == 1)
     start(tail_copy(1, 0, me_sp + 3), (x == 1) & (z < nz - 2))
-    pl.when(rightward == 1)(lambda: send_z(2, middle[-1:]))
+    pl.when((rightward == 1) & (outer | (x == 1)))(lambda: send_z(2, middle[-1:]))
 
     @pl.when((x == 0) & (z < 2))
     def _():

time: 140 us -> 140 us (level)
  no operation moved by 1% of the time
where the time goes in v6:
time: 140 us
  Pallas kernels  138 us (99%)
  local copies, waits for them, and re-layouts  1.77 us (1%)
    pallas_call x1, Pallas kernels, fused(): pl.pallas_call(functools.partial(layer_kernel, sizes), in_specs=[hbm] * 7...  138 us

profile of v6, /device:TPU:21, one launch (start us, length us, event | category | flops | bytes accessed | tf_op | source)
XLA Modules:
  0.0 139.6 jit_solution(1086364416928272989)
XLA Ops:
  0.0 137.8 %shard_map.181 = bf16[384,512]{1,0:T(8,128)(2,1)} custom-call(bf16[384,1024]{1,0:T(8,128)(2,1)} %q_in.1, bf16[384,512]{1,0:T(8,128)(2,1)} %t_in.1, bf16[384,512]{1,0:T(8,128)(2,1)} %latent_in.1, bf16[512,1024]{1,0:T(8,128)(2,1)} %kup_in.1, bf16[512,1024]{1,0:T(8,128)(2,1)} %vup_in.1, bf16[1024,2048]{1,0:T(8,128)(2,1)} %proj_in.1, bf16[384,512]{1,0:T(8,128)(2,1)} %resid_in.1, ...), custom_call_target="tpu_custom_call" | custom-call | tf_op jit(solution)/shard_map/pallas_call | solution.py:1017
  137.8 1.8 %copy.21 = bf16[384,512]{1,0:T(8,128)(2,1)} copy(bf16[384,512]{1,0:T(8,128)(2,1)} %shard_map.181) | data formatting | bytes 786432
